TPU v7x, 32 devices: a whole 2x2x4 slice. The times are simulated.
32 devices in a mesh: sp: 8 (over z, core), tp: 4 (over y, x).
Axes of the slice: x: 2, y: 2, z: 4, core: 2. Of those that a mesh axis runs over, the one named last changes fastest.
Arguments:
- routes: int32 [1536, 2], P('sp'), may hold values from 0 to 7, all different within a row; in each aligned block of 192 rows (0 to 191, 192 to 383, ...) at most 72 rows name the same one
- route_weights: float32 [1536, 2], P('sp'), may hold values from 0.2 to 1
- expert_inputs: bfloat16 [1536, 2048], P('sp', 'tp'), may hold values from -6 to 6
- out_grad: bfloat16 [1536, 2048], P('sp', 'tp'), may hold values from -6 to 6
- w_gate: bfloat16 [8, 2816, 2048], P('sp', 'tp'), may hold values from -0.125 to 0.125
- w_up: bfloat16 [8, 2816, 2048], P('sp', 'tp'), may hold values from -0.125 to 0.125
- w_down: bfloat16 [8, 2816, 2048], P('sp', 'tp'), may hold values from -0.109375 to 0.109375
- conv_u: bfloat16 [1536, 512], P('sp', 'tp'), may hold values from -6 to 6
- conv_b: bfloat16 [1536, 512], P('sp', 'tp'), may hold values from -6 to 6
- conv_c: bfloat16 [1536, 512], P('sp', 'tp'), may hold values from -6 to 6
- conv_taps: float32 [3, 512], P(None, 'tp'), may hold values from -3 to 3
- out_proj: bfloat16 [512, 2048], P('tp'), may hold values from -0.25 to 0.25
Outputs:
- grad_w_gate: bfloat16 [8, 2816, 2048], P('sp', 'tp')
- grad_w_up: bfloat16 [8, 2816, 2048], P('sp', 'tp')
- grad_w_down: bfloat16 [8, 2816, 2048], P('sp', 'tp')
- grad_input: bfloat16 [1536, 2048], P('sp', 'tp')
- grad_proj: float32 [2048, 512], P('sp', 'tp')
- grad_u: bfloat16 [1536, 512], P('sp', 'tp')
- grad_b: bfloat16 [1536, 512], P('sp', 'tp')
- grad_c: bfloat16 [1536, 512], P('sp', 'tp')
Inputs may be any that keep to these rules, and one draw needn't show every extreme that they name: `routes`: each row names two different experts. In each aligned block of 192 rows no expert is named more than 72 times, a bound that some block reaches.
All inputs are finite; a program needn't handle non-finite values.
Results may differ from a plain program's by a relative error of at most 0.025.
Values may be sent and summed in bfloat16 or wider, within the bound.
A program may use at most 64 MiB of HBM per device.

v0:
```python
import functools

import jax
import jax.numpy as jnp
from jax import lax
from jax.experimental import pallas as pl
from jax.experimental.pallas import tpu as pltpu
from jax.sharding import PartitionSpec as P

MESH = pl.DeviceIdType.MESH
F32 = jnp.float32
BF16 = jnp.bfloat16


def contract_first(left, right):
    return lax.dot_general(
        left, right, (((0,), (0,)), ((), ())), preferred_element_type=jnp.float32
    )


def contract_last(left, right):
    return lax.dot_general(
        left, right, (((1,), (1,)), ((), ())), preferred_element_type=jnp.float32
    )


def loop(count, step):
    lax.fori_loop(0, count, lambda i, c: (step(i), c)[1], 0)


def enter(sizes):
    barrier = pltpu.get_barrier_semaphore()
    for axis, size in sizes:
        me = lax.axis_index(axis)

        def greet(i, axis=axis, size=size, me=me):
            pl.semaphore_signal(
                barrier,
                inc=1,
                device_id={axis: lax.rem(me + i + 1, size)},
                device_id_type=MESH,
            )

        loop(size - 1, greet)
    return lambda: pl.semaphore_wait(barrier, sum(size - 1 for _, size in sizes))


def remote(src, dst, send, recv, **where):
    return pltpu.make_async_remote_copy(
        src_ref=src,
        dst_ref=dst,
        send_sem=send,
        recv_sem=recv,
        device_id=where,
        device_id_type=MESH,
    )


def slot_codes(routes, experts):
    count = routes.shape[1]
    names = lax.broadcasted_iota(jnp.int32, (experts, count), 0)
    first = (routes[0:1, :] == names).astype(F32)
    second = (routes[1:2, :] == names).astype(F32)
    early = lax.broadcasted_iota(jnp.int32, (count, count), 0)
    late = lax.broadcasted_iota(jnp.int32, (count, count), 1)
    before = (early < late).astype(F32).astype(BF16)
    rank = jnp.dot((first + second).astype(BF16), before, preferred_element_type=F32)
    code = jnp.where(first + second > 0.5, rank, -1.0).astype(jnp.int32)
    return code, first, second


def dispatch_kernel(
    S, T, routes_ref, wts_ref, xin_ref, gin_ref, x_ref, g_ref,
    xs, gs, zsend, zrecv, fsend, frecv, rsend, rrecv, lsem,
):
    s, p = lax.axis_index("sp"), lax.axis_index("tp")
    cap, d = xs.shape[1], xs.shape[2]
    wait_entry = enter((("sp", S), ("tp", T)))

    code, first, second = slot_codes(routes_ref[...], S)
    weight = first * wts_ref[0:1, :] + second * wts_ref[1:2, :]
    slots = lax.broadcasted_iota(jnp.int32, (cap, code.shape[1]), 0)
    xin = xin_ref[...]
    gin = gin_ref[...]
    for e in range(S):
        mask = slots == code[e : e + 1, :]
        pick = mask.astype(F32).astype(BF16)
        xs[e] = jnp.dot(pick, xin, preferred_element_type=F32).astype(BF16)
        held = jnp.sum(jnp.where(mask, weight[e : e + 1, :], 0.0), axis=1, keepdims=True)
        gs[e] = (held * jnp.dot(pick, gin, preferred_element_type=F32)).astype(BF16)
    wait_entry()

    arrays = ((xs, x_ref), (gs, g_ref))

    def cols(q, half=None):
        if half is None:
            return pl.ds(pl.multiple_of(q * d, d), d)
        return pl.ds(pl.multiple_of(q * d + half * (d // 2), d // 2), d // 2)

    def origin(o):
        return lax.rem(s - o + S, S)

    def zcopy(i, o, arriving=False):
        src, out = arrays[i]
        dst = lax.rem(s + o, S)
        row = origin(o) if arriving else s
        return remote(
            src.at[dst], out.at[row, :, cols(p)], zsend.at[i, o], zrecv.at[i, o], sp=dst
        )

    locals_ = [
        pltpu.make_async_copy(src.at[s], out.at[s, :, cols(p)], lsem.at[i])
        for i, (src, out) in enumerate(arrays)
    ]
    for i in range(2):
        locals_[i].start()
        loop(S - 1, lambda k, i=i: zcopy(i, k + 1).start())

    relay = T == 4
    if relay:
        xn, yn = p + 1 - 2 * lax.rem(p, 2), lax.rem(p + 2, 4)
        partners = ((xn, xn), (yn, yn))
    else:
        partners = tuple(
            (lax.rem(p + r, T), lax.rem(p - r + T, T)) for r in range(1, T)
        )

    def fcopy(i, o, k, arriving=False):
        out = arrays[i][1]
        to, whence = partners[k]
        view = out.at[origin(o), :, cols(whence if arriving else p)]
        return remote(view, view, fsend.at[i, o, k], frecv.at[i, o, k], tp=to)

    def rcopy(i, o, k, arriving=False):
        out = arrays[i][1]
        near, far = ((xn, yn), (yn, xn))[k]
        view = out.at[origin(o), :, cols(3 - p if arriving else near, k)]
        return remote(view, view, rsend.at[i, o, k], rrecv.at[i, o, k], tp=far)

    def forward(i, o):
        @pl.when(o > 0)
        def _():
            zcopy(i, o, True).wait_recv()

        for k in range(len(partners)):
            fcopy(i, o, k).start()

    def pass_on(i, o):
        for k in range(len(partners)):
            fcopy(i, o, k, True).wait_recv()
            if relay:
                rcopy(i, o, k).start()

    for i in range(2):
        locals_[i].wait()
        forward(i, 0)
        if i == 1:
            pass_on(0, S - 1)

        def step(k, i=i):
            forward(i, k + 1)
            pass_on(i, k)

        loop(S - 1, step)
    pass_on(1, S - 1)
    for i in range(2):
        loop(S - 1, lambda k, i=i: zcopy(i, k + 1).wait_send())

        def finish(o, i=i):
            for k in range(len(partners)):
                fcopy(i, o, k).wait_send()
                if relay:
                    rcopy(i, o, k).wait_send()
                    rcopy(i, o, k, True).wait_recv()

        loop(S, finish)


def return_kernel(
    S, T, part_ref, routes_ref, grad_ref, edge_ref, own_ref, full_ref, halo_ref,
    landed, met, passed, summed, back,
    fsend, frecv, bsend, brecv, zsend, zrecv, asend, arecv, hsend, hrecv,
):
    s, p = lax.axis_index("sp"), lax.axis_index("tp")
    cap, d = summed.shape[1], summed.shape[2]
    relay = T == 4
    half = d // 2
    wait_entry = enter((("sp", S), ("tp", T)))
    wait_entry()

    def cols(q):
        return pl.ds(pl.multiple_of(q * d, d), d)

    def halfcols(q, h):
        return pl.ds(pl.multiple_of(q * d + h * half, half), half)

    def block(t):
        return lax.rem(s + t + 1, S)

    def zcopy(t, arriving=False):
        row = lax.rem(s - t - 1 + S, S) if arriving else s
        return remote(
            summed.at[block(t)], back.at[row], zsend.at[t], zrecv.at[t], sp=block(t)
        )

    def hcopy(k):
        to = lax.rem(s + (1 if k == 0 else S - 1), S)
        return remote(
            edge_ref.at[1 - k], halo_ref.at[k], hsend.at[k], hrecv.at[k], sp=to
        )

    if relay:
        xn, yn = p + 1 - 2 * lax.rem(p, 2), lax.rem(p + 2, 4)
        order = ((xn, yn), (yn, xn))

        def fcopy(t, h, k):
            to = order[h][0]
            return remote(
                part_ref.at[block(t), :, halfcols(3 - p if k else to, h)],
                landed.at[h, k, block(t)],
                fsend.at[t, 2 * h + k],
                frecv.at[t, 2 * h + k],
                tp=to,
            )

        def bcopy(t, h):
            return remote(
                passed.at[h, block(t)], met.at[h, block(t)],
                bsend.at[t, h], brecv.at[t, h], tp=order[h][1],
            )

        def start(t):
            for k in (1, 0):
                for h in range(2):
                    fcopy(t, h, k).start()

        def combine(t):
            for h in range(2):
                fcopy(t, h, 1).wait_recv()
                mine = part_ref[block(t), :, halfcols(order[h][1], h)].astype(F32)
                passed[h, block(t)] = (mine + landed[h, 1, block(t)].astype(F32)).astype(
                    BF16
                )

        def total(t, out, row):
            for h in range(2):
                fcopy(t, h, 0).wait_recv()
                bcopy(t, h).wait_recv()
                mine = part_ref[block(t), :, halfcols(p, h)].astype(F32)
                mine = mine + landed[h, 0, block(t)].astype(F32)
                mine = mine + met[h, block(t)].astype(F32)
                out[row, :, h * half : (h + 1) * half] = mine.astype(BF16)

        ahead, lag = min(3, S), 2
    else:

        def fcopy(t, r):
            q = lax.rem(p + r, T)
            return remote(
                part_ref.at[block(t), :, cols(q)],
                landed.at[r - 1, block(t)],
                fsend.at[t, r - 1],
                frecv.at[t, r - 1],
                tp=q,
            )

        def start(t):
            for r in range(1, T):
                fcopy(t, r).start()

        def total(t, out, row):
            for r in range(1, T):
                fcopy(t, r).wait_recv()
            value = part_ref[block(t), :, cols(p)].astype(F32)
            for r in range(1, T):
                value = value + landed[r - 1, block(t)].astype(F32)
            out[row] = value.astype(BF16)

        ahead, lag = S, 0

    loop(ahead, start)
    for k in range(2):
        hcopy(k).start()
    code, _, _ = slot_codes(routes_ref[...], S)
    slots = lax.broadcasted_iota(jnp.int32, (cap, code.shape[1]), 0)

    def step(t):
        if relay:

            @pl.when(t < S)
            def _():
                combine(t)

        @pl.when(jnp.logical_and(t >= lag, t < S - 1 + lag))
        def _():
            total(t - lag, summed, block(t - lag))

        if relay:

            @pl.when(t < S)
            def _():
                for h in range(2):
                    bcopy(t, h).start()

            @pl.when(t + ahead < S)
            def _():
                start(t + ahead)

        @pl.when(t >= lag + 1)
        def _():
            zcopy(t - lag - 1).start()

    loop(S + lag, step)
    total(S - 1, back, s)
    loop(S - 1, lambda t: zcopy(t, True).wait_recv())
    value = jnp.zeros((code.shape[1], d), F32)
    for e in range(S):
        pick = (slots == code[e : e + 1, :]).astype(F32).astype(BF16)
        value = value + contract_first(pick, back[e])
    value = (grad_ref[...].astype(F32) + value).astype(BF16)
    own_ref[...] = value
    full_ref[:, cols(p)] = value
    loop(S - 1, lambda t: zcopy(t).wait_send())

    def acopy(r, arriving=False):
        at = lax.rem(p - r + T, T) if arriving else p
        return remote(
            own_ref, full_ref.at[:, cols(at)], asend.at[r - 1], arecv.at[r - 1],
            tp=lax.rem(p + r, T),
        )

    for r in range(1, T):
        acopy(r).start()

    def finish(t):
        if relay:
            for h in range(2):
                fcopy(t, h, 0).wait_send()
                fcopy(t, h, 1).wait_send()
                bcopy(t, h).wait_send()
        else:
            for r in range(1, T):
                fcopy(t, r).wait_send()

    loop(S, finish)
    for k in range(2):
        hcopy(k).wait()
    for r in range(1, T):
        acopy(r).wait_send()
        acopy(r, True).wait_recv()


def reduce_kernel(
    S, proj_ref, edge_ref, sum_ref, halo_ref,
    given, pairs, landed, gsend, grecv, psend, precv, hsend, hrecv,
):
    s = lax.axis_index("sp")
    n = S // 2
    z, c = s // 2, lax.rem(s, 2)
    enter((("sp", S),))()

    def hcopy(k):
        to = lax.rem(s + (1 if k == 0 else S - 1), S)
        return remote(
            edge_ref.at[1 - k], halo_ref.at[k], hsend.at[k], hrecv.at[k], sp=to
        )

    def at(o):
        return lax.rem(z + o, n)

    def gcopy(o):
        return remote(
            proj_ref.at[2 * at(o) + 1 - c], given.at[at(o)],
            gsend.at[o], grecv.at[o], sp=s + 1 - 2 * c,
        )

    def pcopy(o):
        return remote(
            pairs.at[at(o)], landed.at[o - 1], psend.at[o - 1], precv.at[o - 1],
            sp=2 * at(o) + c,
        )

    for k in range(2):
        hcopy(k).start()
    for o in range(1, n + 1):
        gcopy(o % n).start()

    def pair(o):
        gcopy(o).wait_recv()
        return proj_ref[2 * at(o) + c].astype(F32) + given[at(o)].astype(F32)

    for o in range(1, n):
        pairs[at(o)] = pair(o).astype(BF16)
        if o > 1:
            pcopy(o - 1).start()
    sum_ref[...] = pair(0)
    pcopy(n - 1).start()
    for o in range(1, n):
        pcopy(o).wait_recv()
        sum_ref[...] += landed[o - 1].astype(F32)
    for o in range(n):
        gcopy(o).wait_send()
        if o > 0:
            pcopy(o).wait_send()
    for k in range(2):
        hcopy(k).wait()


def vmem(count):
    return [pl.BlockSpec(memory_space=pltpu.VMEM)] * count


def params(number):
    return pltpu.CompilerParams(collective_id=number, has_side_effects=True)


def rimmed(value, halo):
    s, size = lax.axis_index("sp"), lax.axis_size("sp")
    before = jnp.where(s > 0, halo[0, -1:], 0.0)
    after = jnp.where(s < size - 1, halo[1, :1], 0.0)
    return jnp.concatenate([before, value, after], axis=0)


def edges(value):
    return jnp.stack([value[:8], value[-8:]])


def body(
    routes, route_weights, expert_inputs, out_grad, w_gate, w_up, w_down,
    conv_u, conv_b, conv_c, conv_taps, out_proj,
):
    S, T = lax.axis_size("sp"), lax.axis_size("tp")
    tokens, d = expert_inputs.shape
    channels = conv_u.shape[1]
    cap = 3 * tokens // S
    dma = pltpu.SemaphoreType.DMA
    sent = jax.ShapeDtypeStruct((S, cap, T * d), BF16)
    ways = 2 if T == 4 else T - 1
    relays = (2, S, 2) if T == 4 else (1, 1, 1)
    rows, grads = pl.pallas_call(
        functools.partial(dispatch_kernel, S, T),
        out_shape=(sent, sent),
        in_specs=vmem(4),
        out_specs=tuple(vmem(2)),
        scratch_shapes=[
            pltpu.VMEM((S, cap, d), BF16),
            pltpu.VMEM((S, cap, d), BF16),
            dma((2, S)),
            dma((2, S)),
            dma((2, S, ways)),
            dma((2, S, ways)),
            dma(relays),
            dma(relays),
            dma((2,)),
        ],
        compiler_params=params(0),
        name="dispatch",
    )(routes.T, route_weights.T, expert_inputs, out_grad)
    rows = rows.reshape(S * cap, T * d)
    grads = grads.reshape(S * cap, T * d)

    gate_weight, up_weight, down_weight = w_gate[0], w_up[0], w_down[0]
    gate_pre = contract_last(rows, gate_weight)
    up_pre = contract_last(rows, up_weight)
    sigma = jax.nn.sigmoid(gate_pre)
    gate_act = gate_pre * sigma
    hidden = (gate_act * up_pre).astype(BF16)
    grad_hidden = contract_last(grads, down_weight)
    gate_back = (
        grad_hidden * up_pre * sigma * (1.0 + gate_pre * (1.0 - sigma))
    ).astype(BF16)
    up_back = (grad_hidden * gate_act).astype(BF16)
    grad_down = contract_first(hidden, grads).astype(BF16)
    grad_gate = contract_first(gate_back, rows).astype(BF16)
    grad_up = contract_first(up_back, rows).astype(BF16)
    partial_value = jnp.dot(gate_back, gate_weight, preferred_element_type=F32) + jnp.dot(
        up_back, up_weight, preferred_element_type=F32
    )
    partial_value = partial_value.astype(BF16).reshape(S, cap, T * d)

    if T == 4:
        pieces = 4
        shapes = ((2, 2, S, cap, d // 2), (2, S, cap, d // 2), (2, S, cap, d // 2))
    else:
        pieces = T - 1
        shapes = ((T - 1, S, cap, d), (8, 128), (8, 128))
    landing = [pltpu.VMEM(shape, BF16) for shape in shapes]
    mixed_in = conv_c.astype(F32) * conv_u.astype(F32)
    halo_shape = jax.ShapeDtypeStruct((2, 8, channels), F32)
    grad_input, grad_full, halo = pl.pallas_call(
        functools.partial(return_kernel, S, T),
        out_shape=(
            jax.ShapeDtypeStruct((tokens, d), BF16),
            jax.ShapeDtypeStruct((tokens, T * d), BF16),
            halo_shape,
        ),
        in_specs=vmem(4),
        out_specs=tuple(vmem(3)),
        scratch_shapes=[
            *landing,
            pltpu.VMEM((S, cap, d), BF16),
            pltpu.VMEM((S, cap, d), BF16),
            dma((S, pieces)),
            dma((S, pieces)),
            dma(relays[1:]),
            dma(relays[1:]),
            dma((S,)),
            dma((S,)),
            dma((T - 1,)),
            dma((T - 1,)),
            dma((2,)),
            dma((2,)),
        ],
        compiler_params=params(1),
        name="bring_back",
    )(partial_value, routes.T, out_grad, edges(mixed_in))

    padded = rimmed(mixed_in, halo)
    convolved = (
        conv_taps[0] * padded[0:tokens]
        + conv_taps[1] * padded[1 : tokens + 1]
        + conv_taps[2] * padded[2 : tokens + 2]
    )
    conv_out = (conv_b.astype(F32) * convolved).astype(BF16)
    grad_conv = contract_last(grad_full, out_proj)
    grad_b = (grad_conv * convolved).astype(BF16)
    grad_mixed = grad_conv * conv_b.astype(F32)
    proj = contract_first(grad_full, conv_out).astype(BF16)
    width = proj.shape[0] // S
    proj_sum, halo = pl.pallas_call(
        functools.partial(reduce_kernel, S),
        out_shape=(jax.ShapeDtypeStruct((width, channels), F32), halo_shape),
        in_specs=vmem(2),
        out_specs=tuple(vmem(2)),
        scratch_shapes=[
            pltpu.VMEM((S // 2, width, channels), BF16),
            pltpu.VMEM((S // 2, width, channels), BF16),
            pltpu.VMEM((S // 2 - 1, width, channels), BF16),
            dma((S // 2,)),
            dma((S // 2,)),
            dma((S // 2 - 1,)),
            dma((S // 2 - 1,)),
            dma((2,)),
            dma((2,)),
        ],
        compiler_params=params(2),
        name="sum_proj",
    )(proj.reshape(S, width, channels), edges(grad_mixed))
    rim = rimmed(grad_mixed, halo)
    grad_z = (
        conv_taps[0] * rim[2 : tokens + 2]
        + conv_taps[1] * rim[1 : tokens + 1]
        + conv_taps[2] * rim[0:tokens]
    )
    grad_c = (grad_z * conv_u.astype(F32)).astype(BF16)
    grad_u = (grad_z * conv_c.astype(F32)).astype(BF16)
    return (
        grad_gate[None], grad_up[None], grad_down[None], grad_input, proj_sum,
        grad_u, grad_b, grad_c,
    )


def solution(mesh):
    in_specs = (
        P("sp", None),
        P("sp", None),
        P("sp", "tp"),
        P("sp", "tp"),
        P("sp", "tp", None),
        P("sp", "tp", None),
        P("sp", "tp", None),
        P("sp", "tp"),
        P("sp", "tp"),
        P("sp", "tp"),
        P(None, "tp"),
        P("tp", None),
    )
    out_specs = (
        P("sp", "tp", None),
        P("sp", "tp", None),
        P("sp", "tp", None),
        P("sp", "tp"),
        P("sp", "tp"),
        P("sp", "tp"),
        P("sp", "tp"),
        P("sp", "tp"),
    )
    return jax.shard_map(body, mesh=mesh, in_specs=in_specs, out_specs=out_specs, check_vma=False)
```

profile of v0, /device:TPU:0, one launch (start us, length us, event | category | flops | bytes accessed | tf_op | source)
XLA Modules:
  0.0 154.3 jit_solution(17056196496389727305)
XLA Ops:
  0.6 0.0 copy-start
  0.6 54.0 %dispatch.1 = (bf16[8,72,2048]{2,1,0:T(8,128)(2,1)}, bf16[8,72,2048]{2,1,0:T(8,128)(2,1)}) custom-call(s32[2,192]{1,0:T(2,128)} %bitcast.64, f32[2,192]{1,0:T(2,128)} %bitcast.66, bf16[192,512]{1,0:T(8,128)(2,1)} %xin_ref.1, bf16[192,512]{1,0:T(8,128)(2,1)} %grad_ref.1), custom_call_target="tpu_custom_call" | custom-call | tf_op jit(solution)/shard_map/dispatch/pallas_call | solution.py:440
  54.6 0.0 copy-done
  54.6 0.0 copy-start.10
  54.6 0.0 copy-start.12
  54.7 3.9 %fusion.5 = f32[576,704]{1,0:T(8,128)S(1)} fusion(bf16[576,2048]{1,0:T(8,128)(2,1)} %bitcast.69, bf16[1,704,2048]{2,1,0:T(8,128)(2,1)S(1)} %copy-done), kind=kOutput, calls=%fused_computation.9 | convolution fusion | flops 1660944384 | bytes 6864896 | tf_op jit(solution)/shard_map/dot_general | solution.py:22
  58.5 0.0 copy-start.9
  58.6 2.0 %fusion.8 = f32[576,704]{1,0:T(8,128)S(1)} fusion(bf16[576,2048]{1,0:T(8,128)(2,1)S(1)} %bitcast.70, bf16[1,704,2048]{2,1,0:T(8,128)(2,1)S(1)} %copy-done.10), kind=kOutput, calls=%fused_computation.12 | convolution fusion | flops 1660944384 | bytes 6864896 | tf_op jit(solution)/shard_map/dot_general | solution.py:22
  60.6 0.5 copy-done.11
  61.1 2.5 %multiply_convert_fusion.1 = (bf16[576,704]{1,0:T(8,128)(2,1)S(1)}, bf16[576,704]{1,0:T(8,128)(2,1)S(1)}) fusion(f32[576,704]{1,0:T(8,128)S(1)} %fusion.5, f32[576,704]{1,0:T(8,128)S(1)} %fusion.8, bf16[576,2048]{1,0:T(8,128)(2,1)S(1)} %bitcast.67, bf16[1,704,2048]{2,1,0:T(8,128)(2,1)S(1)} %copy-done.9), kind=kOutput, calls=%fused_computation.18 | convolution fusion | flops 1666215936 | bytes 10108928 | tf_op jit(solution)/shard_map/dot_general | solution.py:22
  63.5 4.0 %fusion = bf16[1,704,2048]{2,1,0:T(8,128)(2,1)} fusion(bf16[576,704]{1,0:T(8,128)(2,1)S(1)} %get-tuple-element.23, bf16[576,2048]{1,0:T(8,128)(2,1)S(1)} %bitcast.71), kind=kOutput, calls=%fused_computation.4 | convolution fusion | flops 1662386176 | bytes 6053888 | tf_op jit(solution)/shard_map/dot_general | solution.py:16
  67.6 4.0 %fusion.1 = bf16[1,704,2048]{2,1,0:T(8,128)(2,1)} fusion(bf16[576,704]{1,0:T(8,128)(2,1)S(1)} %get-tuple-element.22, bf16[576,2048]{1,0:T(8,128)(2,1)S(1)} %bitcast.72), kind=kOutput, calls=%fused_computation.5 | convolution fusion | flops 1662386176 | bytes 6053888 | tf_op jit(solution)/shard_map/dot_general | solution.py:16
  71.6 4.3 %fusion.2 = bf16[1,704,2048]{2,1,0:T(8,128)(2,1)} fusion(bf16[576,2048]{1,0:T(8,128)(2,1)S(1)} %bitcast.68, f32[576,704]{1,0:T(8,128)S(1)} %fusion.8, f32[576,704]{1,0:T(8,128)S(1)} %fusion.5), kind=kOutput, calls=%fused_computation.6 | convolution fusion | flops 1664819200 | bytes 8486912 | tf_op jit(solution)/shard_map/dot_general | solution.py:16
  75.9 2.0 %fusion.3 = f32[576,2048]{1,0:T(8,128)S(1)} fusion(bf16[576,704]{1,0:T(8,128)(2,1)S(1)} %get-tuple-element.23, bf16[1,704,2048]{2,1,0:T(8,128)(2,1)S(1)} %copy-done), kind=kOutput, calls=%fused_computation.7 | convolution fusion | flops 1660944384 | bytes 8413184 | tf_op jit(solution)/shard_map/dot_general | solution.py:476
  77.9 0.0 copy-start.4
  77.9 0.0 copy-start.5
  77.9 3.4 %add_convert_fusion = bf16[576,2048]{1,0:T(8,128)(2,1)} fusion(f32[576,2048]{1,0:T(8,128)S(1)} %fusion.3, bf16[576,704]{1,0:T(8,128)(2,1)S(1)} %get-tuple-element.22, bf16[1,704,2048]{2,1,0:T(8,128)(2,1)S(1)} %copy-done.10), kind=kOutput, calls=%fused_computation | convolution fusion | flops 1663303680 | bytes 10772480 | tf_op jit(solution)/shard_map/dot_general | solution.py:476
  81.4 0.6 pad_maximum_fusion.4.edge_ref
  82.0 44.9 %bring_back.1 = (bf16[192,512]{1,0:T(8,128)(2,1)}, bf16[192,2048]{1,0:T(8,128)(2,1)}, f32[2,8,128]{2,1,0:T(8,128)}) custom-call(bf16[8,72,2048]{2,1,0:T(8,128)(2,1)} %bitcast.62, s32[2,192]{1,0:T(2,128)} %bitcast.65, bf16[192,512]{1,0:T(8,128)(2,1)} %grad_ref.1, f32[2,8,128]{2,1,0:T(8,128)} %pad_maximum_fusion.4.edge_ref), custom_call_target="tpu_custom_call" | custom-call | tf_op jit(solution)/shard_map/bring_back/pallas_call | solution.py:490
  126.9 0.7 fusion.27
  127.6 0.8 slice_bitcast_fusion.6
  128.4 0.0 copy-done.3
  128.4 2.4 %convolution_convert_fusion.3 = bf16[2048,128]{1,0:T(8,128)(2,1)} fusion(bf16[192,2048]{1,0:T(8,128)(2,1)} %get-tuple-element.18, bf16[192,128]{1,0:T(8,128)(2,1)S(1)} %copy-done.3, f32[1,128]{1,0:T(1,128)S(1)} %get-tuple-element.35, f32[192,128]{1,0:T(8,128)S(1)} %convert_multiply_fusion.3, f32[1,128]{1,0:T(1,128)S(1)} %get-tuple-element.34, ...), kind=kOutput, calls=%fused_computation.16 | convolution fusion | flops 101171200 | bytes 1460736 | tf_op jit(solution)/shard_map/dot_general | solution.py:16
  130.8 2.1 %multiply_convert_fusion.4 = (bf16[192,128]{1,0:T(8,128)(2,1)}, f32[192,128]{1,0:T(8,128)S(1)}) fusion(f32[1,128]{1,0:T(1,128)S(1)} %get-tuple-element.35, f32[192,128]{1,0:T(8,128)S(1)} %convert_multiply_fusion.3, f32[128]{0:T(128)S(1)} %get-tuple-element.37, f32[128]{0:T(128)S(1)} %get-tuple-element.38, f32[1,128]{1,0:T(1,128)S(1)} %get-tuple-element.34, ...), kind=kOutput, calls=%fused_computation.42 | convolution fusion | flops 100933632 | bytes 1608192 | tf_op jit(solution)/shard_map/dot_general | solution.py:22
  132.9 0.6 copy-done.2
  133.6 0.0 copy-done.6
  133.6 0.6 pad_maximum_fusion.5.edge_ref
  134.2 14.4 %sum_proj.1 = (f32[256,128]{1,0:T(8,128)}, f32[2,8,128]{2,1,0:T(8,128)}) custom-call(bf16[8,256,128]{2,1,0:T(8,128)(2,1)} %bitcast.63, f32[2,8,128]{2,1,0:T(8,128)} %pad_maximum_fusion.5.edge_ref), custom_call_target="tpu_custom_call" | custom-call | tf_op jit(solution)/shard_map/sum_proj/pallas_call | solution.py:530
  148.6 0.7 fusion.30
  149.3 1.7 %fusion.15 = (bf16[192,128]{1,0:T(8,128)(2,1)}, bf16[192,128]{1,0:T(8,128)(2,1)}) fusion(bf16[192,128]{1,0:T(8,128)(2,1)} %param.19, f32[192,128]{1,0:T(8,128)} %copy-done.2, f32[1,128]{1,0:T(1,128)S(1)} %get-tuple-element.33, f32[128]{0:T(128)} %copy-done.7, f32[128]{0:T(128)} %copy-done.8, f32[1,128]{1,0:T(1,128)S(1)} %get-tuple-element.32, ...), kind=kLoop, calls=%fused_computation.28 | loop fusion | flops 319488 | bytes 297472 | tf_op jit(solution)/shard_map/convert_element_type | solution.py:555
  151.1 1.6 %copy.22 = bf16[192,512]{1,0:T(8,128)(2,1)} copy(bf16[192,512]{1,0:T(8,128)(2,1)} %get-tuple-element.50) | data formatting | bytes 393216
  152.7 1.6 %copy.23 = f32[256,128]{1,0:T(8,128)} copy(f32[256,128]{1,0:T(8,128)} %get-tuple-element.51) | data formatting | bytes 262144
  (18 shorter events, 0.0 us)
Async XLA Ops:
  0.6 54.0 %copy-start = (bf16[1,704,2048]{2,1,0:T(8,128)(2,1)S(1)}, bf16[1,704,2048]{2,1,0:T(8,128)(2,1)}, u32[]{:S(2)}) copy-start(bf16[1,704,2048]{2,1,0:T(8,128)(2,1)} %param.16) | copy-start | bytes 8650756
  54.6 3.9 %copy-start.10 = (bf16[1,704,2048]{2,1,0:T(8,128)(2,1)S(1)}, bf16[1,704,2048]{2,1,0:T(8,128)(2,1)}, u32[]{:S(2)}) copy-start(bf16[1,704,2048]{2,1,0:T(8,128)(2,1)} %param.17) | copy-start | bytes 8650756
  54.6 3.9 %copy-start.12 = (bf16[8,72,2048]{2,1,0:T(8,128)(2,1)S(1)}, bf16[8,72,2048]{2,1,0:T(8,128)(2,1)}, u32[]{:S(2)}) copy-start(bf16[8,72,2048]{2,1,0:T(8,128)(2,1)} %get-tuple-element.16) | copy-start | bytes 7077892
  58.5 2.1 %copy-start.9 = (bf16[1,704,2048]{2,1,0:T(8,128)(2,1)S(1)}, bf16[1,704,2048]{2,1,0:T(8,128)(2,1)}, u32[]{:S(2)}) copy-start(bf16[1,704,2048]{2,1,0:T(8,128)(2,1)} %param.18) | copy-start | bytes 8650756
  58.5 2.5 %copy-start.11 = (bf16[8,72,2048]{2,1,0:T(8,128)(2,1)S(1)}, bf16[8,72,2048]{2,1,0:T(8,128)(2,1)}, u32[]{:S(2)}) copy-start(bf16[8,72,2048]{2,1,0:T(8,128)(2,1)} %get-tuple-element.15) | copy-start | bytes 7077892
  77.9 3.5 %copy-start.4 = (bf16[192,128]{1,0:T(8,128)(2,1)S(1)}, bf16[192,128]{1,0:T(8,128)(2,1)}, u32[]{:S(2)}) copy-start(bf16[192,128]{1,0:T(8,128)(2,1)} %param.19) | copy-start | bytes 147460
  77.9 3.5 %copy-start.5 = (bf16[192,128]{1,0:T(8,128)(2,1)S(1)}, bf16[192,128]{1,0:T(8,128)(2,1)}, u32[]{:S(2)}) copy-start(bf16[192,128]{1,0:T(8,128)(2,1)} %param.21) | copy-start | bytes 147460
  81.3 47.0 %copy-start.3 = (bf16[192,128]{1,0:T(8,128)(2,1)S(1)}, bf16[192,128]{1,0:T(8,128)(2,1)}, u32[]{:S(2)}) copy-start(bf16[192,128]{1,0:T(8,128)(2,1)} %param.20) | copy-start | bytes 147460
  81.3 49.5 %copy-start.1 = (bf16[128,2048]{1,0:T(8,128)(2,1)S(1)}, bf16[128,2048]{1,0:T(8,128)(2,1)}, u32[]{:S(2)}) copy-start(bf16[128,2048]{1,0:T(8,128)(2,1)} %param.23) | copy-start | bytes 1572868
  128.4 5.2 %copy-start.6 = (f32[128]{0:T(128)}, f32[128]{0:T(128)S(1)}, u32[]{:S(2)}) copy-start(f32[128]{0:T(128)S(1)} %get-tuple-element.36) | copy-start | bytes 1540
  128.4 5.2 %copy-start.7 = (f32[128]{0:T(128)}, f32[128]{0:T(128)S(1)}, u32[]{:S(2)}) copy-start(f32[128]{0:T(128)S(1)} %get-tuple-element.37) | copy-start | bytes 1540
  128.4 5.2 %copy-start.8 = (f32[128]{0:T(128)}, f32[128]{0:T(128)S(1)}, u32[]{:S(2)}) copy-start(f32[128]{0:T(128)S(1)} %get-tuple-element.38) | copy-start | bytes 1540
  132.9 0.6 copy-start.2
where the time goes:
time: 155 us; the launch traced here: 154 us
  Pallas kernels  113 us (73%)
  matrix products  30.7 us (20%)
  local copies, waits for them, and re-layouts  5.16 us (3%)
  other arithmetic  4.34 us (3%)
    pallas_call x1, Pallas kernels, body(): pl.pallas_call(functools.partial(dispatch_kernel, S, T), out_shape=(sent,...  54 us
    pallas_call x1, Pallas kernels, body(): pl.pallas_call(functools.partial(return_kernel, S, T), out_shape=(jax.Sha...  44.9 us
    dot_general x4, matrix products, contract_first(): lax.dot_general(left, right, (((0,), (0,)), ((), ())), preferred_element_...  14.8 us
    pallas_call x1, Pallas kernels, body(): pl.pallas_call(functools.partial(reduce_kernel, S), out_shape=(jax.ShapeD...  14.4 us
    dot_general x4, matrix products, contract_last(): lax.dot_general(left, right, (((1,), (1,)), ((), ())), preferred_element_...  10.5 us
    unnamed x28, local copies, waits for them, and re-layouts  4.36 us
    dot_general x1, matrix products, body(): jnp.dot(up_back, up_weight, preferred_element_type=F32)  3.44 us

commit v1 on v0

v1 whole, which is shorter than its diff:
```python
import functools

import jax
import jax.numpy as jnp
from jax import lax
from jax.experimental import pallas as pl
from jax.experimental.pallas import tpu as pltpu
from jax.sharding import PartitionSpec as P

MESH = pl.DeviceIdType.MESH
F32 = jnp.float32
BF16 = jnp.bfloat16


def contract_first(left, right):
    return lax.dot_general(
        left, right, (((0,), (0,)), ((), ())), preferred_element_type=jnp.float32
    )


def contract_last(left, right):
    return lax.dot_general(
        left, right, (((1,), (1,)), ((), ())), preferred_element_type=jnp.float32
    )


def loop(count, step):
    lax.fori_loop(0, count, lambda i, c: (step(i), c)[1], 0)


def enter(sizes):
    barrier = pltpu.get_barrier_semaphore()
    for axis, size in sizes:
        me = lax.axis_index(axis)

        def greet(i, axis=axis, size=size, me=me):
            pl.semaphore_signal(
                barrier,
                inc=1,
                device_id={axis: lax.rem(me + i + 1, size)},
                device_id_type=MESH,
            )

        loop(size - 1, greet)
    return lambda: pl.semaphore_wait(barrier, sum(size - 1 for _, size in sizes))


def remote(src, dst, send, recv, **where):
    return pltpu.make_async_remote_copy(
        src_ref=src,
        dst_ref=dst,
        send_sem=send,
        recv_sem=recv,
        device_id=where,
        device_id_type=MESH,
    )


def slot_codes(routes, experts):
    count = routes.shape[1]
    names = lax.broadcasted_iota(jnp.int32, (experts, count), 0)
    first = (routes[0:1, :] == names).astype(F32)
    second = (routes[1:2, :] == names).astype(F32)
    early = lax.broadcasted_iota(jnp.int32, (count, count), 0)
    late = lax.broadcasted_iota(jnp.int32, (count, count), 1)
    before = (early < late).astype(F32).astype(BF16)
    rank = jnp.dot((first + second).astype(BF16), before, preferred_element_type=F32)
    code = jnp.where(first + second > 0.5, rank, -1.0).astype(jnp.int32)
    return code, first, second


def padded_rows(cap):
    return -(-cap // 16) * 16


def expert_kernel(
    S, T, routes_ref, wts_ref, xin_ref, gin_ref, edge_ref, gate_hbm, up_hbm, down_hbm,
    own_ref, full_ref, halo_ref, dgate_ref, dup_ref, ddown_ref,
    gate_w, up_w, down_w, code_ref, weight_ref, zs, xg, xc, pre, upre,
    hid, gback, uback, hid_t, gback_t, uback_t, part, landed, met, passed, summed, back, total_ref,
    wsem, zsend, zrecv, fsend, frecv, rsend, rrecv,
    tsend, trecv, bsend, brecv, ysend, yrecv, asend, arecv, hsend, hrecv,
):
    s, p = lax.axis_index("sp"), lax.axis_index("tp")
    n = S // 2
    z, c = s // 2, lax.rem(s, 2)
    cap, d = summed.shape[1], summed.shape[2]
    capp = padded_rows(cap)
    half = d // 2
    relay = T == 4
    wait_entry = enter((("sp", S), ("tp", T)))

    weights = [
        pltpu.make_async_copy(src.at[0], dst, wsem.at[i])
        for i, (src, dst) in enumerate(((gate_hbm, gate_w), (up_hbm, up_w), (down_hbm, down_w)))
    ]
    for w in weights:
        w.start()

    def offset(q):
        odd = lax.rem(q, 2)
        return lax.rem(odd * ((q + 1) // 2) + (1 - odd) * (n - q // 2), n)

    def dest(j):
        return 2 * lax.rem(z + offset(j // 2), n) + lax.rem(c + j, 2)

    def origin(j):
        return 2 * lax.rem(z - offset(j // 2) + n, n) + lax.rem(c + j, 2)

    def cols(q):
        return pl.ds(pl.multiple_of(q * d, d), d)

    def halfcols(q, h):
        return pl.ds(pl.multiple_of(q * d + h * half, half), half)

    if relay:
        xn, yn = p + 1 - 2 * lax.rem(p, 2), lax.rem(p + 2, 4)
        partners = ((xn, xn), (yn, yn))
        order = ((xn, yn), (yn, xn))
    else:
        xn, yn = p, p
        partners = tuple(
            (lax.rem(p + r, T), lax.rem(p - r + T, T)) for r in range(1, T)
        )

    code, first, second = slot_codes(routes_ref[...], S)
    code_ref[...] = code
    weight_ref[...] = first * wts_ref[0:1, :] + second * wts_ref[1:2, :]
    slots = lax.broadcasted_iota(jnp.int32, (cap, code.shape[1]), 0)

    def pick(j):
        to = dest(j)
        mask = slots == code_ref[pl.ds(to, 1), :]
        chosen = mask.astype(F32).astype(BF16)
        zs[0, to] = jnp.dot(chosen, xin_ref[...], preferred_element_type=F32).astype(BF16)
        held = jnp.sum(
            jnp.where(mask, weight_ref[pl.ds(to, 1), :], 0.0), axis=1, keepdims=True
        )
        zs[1, to] = (held * jnp.dot(chosen, gin_ref[...], preferred_element_type=F32)).astype(BF16)

    def zcopy(i, j, arriving=False):
        to = dest(j)
        row = origin(j) if arriving else s
        return remote(
            zs.at[i, to], xg.at[i, row, :, cols(p)], zsend.at[i, j], zrecv.at[i, j], sp=to
        )

    def fcopy(i, j, k, arriving=False):
        to, whence = partners[k]
        view = xg.at[i, origin(j), :, cols(whence if arriving else p)]
        return remote(view, view, fsend.at[i, j, k], frecv.at[i, j, k], tp=to)

    def rcopy(i, j, k, arriving=False):
        near, far = ((xn, yn), (yn, xn))[k]
        view = xg.at[i, origin(j), :, halfcols(3 - p if arriving else near, k)]
        return remote(view, view, rsend.at[i, j, k], rrecv.at[i, j, k], tp=far)

    def spread(i, j):
        for k in range(len(partners)):
            fcopy(i, j, k).start()

    def forward(i, j):
        zcopy(i, j, True).wait_recv()
        spread(i, j)

    def pass_on(i, j):
        for k in range(len(partners)):
            fcopy(i, j, k, True).wait_recv()
            if relay:
                rcopy(i, j, k).start()

    def ready(i, q):
        for b in range(2):
            j = 2 * q + b
            if relay:
                for k in range(2):
                    rcopy(i, j, k, True).wait_recv()
            xc[i, pl.ds(pl.multiple_of(j * capp, capp), cap), :] = xg[i, origin(j)]

    def zback(j, arriving=False):
        row = dest(j) if arriving else s
        return remote(
            summed.at[j], back.at[row], ysend.at[j], yrecv.at[j], sp=origin(j)
        )

    if relay:

        def tcopy(j, h, k):
            to = order[h][0]
            return remote(
                part.at[j, :, halfcols(3 - p if k else to, h)],
                landed.at[h, k, j],
                tsend.at[j, 2 * h + k],
                trecv.at[j, 2 * h + k],
                tp=to,
            )

        def bcopy(j, h):
            return remote(
                passed.at[h, j], met.at[h, j], bsend.at[j, h], brecv.at[j, h], tp=order[h][1]
            )

        def give(j):
            for k in (1, 0):
                for h in range(2):
                    tcopy(j, h, k).start()

        def combine(j):
            for h in range(2):
                tcopy(j, h, 1).wait_recv()
                mine = part[j, :, halfcols(order[h][1], h)].astype(F32)
                passed[h, j] = (mine + landed[h, 1, j].astype(F32)).astype(BF16)

        def total(j, out, row):
            for h in range(2):
                tcopy(j, h, 0).wait_recv()
                bcopy(j, h).wait_recv()
                mine = part[j, :, halfcols(p, h)].astype(F32)
                mine = mine + landed[h, 0, j].astype(F32)
                mine = mine + met[h, j].astype(F32)
                out[row, :, h * half : (h + 1) * half] = mine.astype(BF16)

    else:

        def tcopy(j, r):
            q = lax.rem(p + r, T)
            return remote(
                part.at[j, :, cols(q)],
                landed.at[r - 1, j],
                tsend.at[j, r - 1],
                trecv.at[j, r - 1],
                tp=q,
            )

        def give(j):
            for r in range(1, T):
                tcopy(j, r).start()

        def total(j, out, row):
            for r in range(1, T):
                tcopy(j, r).wait_recv()
            value = part[j, :, cols(p)].astype(F32)
            for r in range(1, T):
                value = value + landed[r - 1, j].astype(F32)
            out[row] = value.astype(BF16)

    lag = 2

    def block(r):
        return lax.rem(r + 2, S)

    def service(t):
        if relay:

            @pl.when(t < S)
            def _():
                combine(block(t))

        @pl.when(jnp.logical_and(jnp.logical_and(t >= lag, t < S + lag), t - lag != S - 2))
        def _():
            total(block(t - lag), summed, block(t - lag))

        @pl.when(t - lag == S - 2)
        def _():
            total(0, back, s)

        if relay:

            @pl.when(t < S)
            def _():
                for h in range(2):
                    bcopy(block(t), h).start()

        @pl.when(jnp.logical_and(t >= lag + 1, t - lag - 1 != S - 2))
        def _():
            zback(block(t - lag - 1)).start()

    def give_chunk(q):
        give(2 * q)
        give(2 * q + 1)

    pick(0)
    xg[0, s, :, cols(p)] = zs[0, s]
    xg[1, s, :, cols(p)] = zs[1, s]
    pick(1)
    xc[...] = jnp.zeros_like(xc)
    wait_entry()
    for i in range(2):
        spread(i, 0)

    def send_picked(k):
        @pl.when(k + 2 < S)
        def _():
            pick(k + 2)

        for i in range(2):
            zcopy(i, k + 1).start()

    loop(S - 1, send_picked)

    def hcopy(k):
        to = lax.rem(s + (1 if k == 0 else S - 1), S)
        return remote(
            edge_ref.at[1 - k], halo_ref.at[k], hsend.at[k], hrecv.at[k], sp=to
        )

    for k in range(2):
        hcopy(k).start()

    def chunk(q):
        return pl.ds(pl.multiple_of(q * 2 * capp, 2 * capp), 2 * capp)

    def step(q):
        live, later, last = q < n, q > 0, q == n

        @pl.when(jnp.logical_and(live, later))
        def _():
            forward(0, 2 * q)

        @pl.when(later)
        def _():
            pass_on(1, 2 * q - 1)

        @pl.when(last)
        def _():
            give_chunk(n - 2)
            service(0)

        @pl.when(later)
        def _():
            ready(0, q - 1)

            @pl.when(q == 1)
            def _():
                for w in weights:
                    w.wait()

            pre[...] = contract_last(xc[0, chunk(q - 1), :], gate_w[...])

        @pl.when(live)
        def _():
            forward(0, 2 * q + 1)
            pass_on(0, 2 * q)

        @pl.when(last)
        def _():
            service(1)

        @pl.when(later)
        def _():
            upre[...] = contract_last(xc[0, chunk(q - 1), :], up_w[...])

        @pl.when(jnp.logical_and(live, later))
        def _():
            forward(1, 2 * q)

        @pl.when(live)
        def _():
            pass_on(0, 2 * q + 1)

        @pl.when(last)
        def _():
            service(2)

        @pl.when(later)
        def _():
            ready(1, q - 1)
            grad_hidden = contract_last(xc[1, chunk(q - 1), :], down_w[...])
            gate_pre, up_pre = pre[...], upre[...]
            sigma = jax.nn.sigmoid(gate_pre)
            gate_act = gate_pre * sigma
            hid[chunk(q - 1), :] = (gate_act * up_pre).astype(BF16)
            gback[chunk(q - 1), :] = (
                grad_hidden * up_pre * sigma * (1.0 + gate_pre * (1.0 - sigma))
            ).astype(BF16)
            uback[chunk(q - 1), :] = (grad_hidden * gate_act).astype(BF16)

        @pl.when(live)
        def _():
            forward(1, 2 * q + 1)
            pass_on(1, 2 * q)

        @pl.when(last)
        def _():
            service(3)

        @pl.when(later)
        def _():
            def piece(f):
                value = jnp.dot(
                    gback[chunk(q - 1), :], gate_w[:, cols(f)], preferred_element_type=F32
                ) + jnp.dot(
                    uback[chunk(q - 1), :], up_w[:, cols(f)], preferred_element_type=F32
                )
                for b in range(2):
                    part[2 * (q - 1) + b, :, cols(f)] = value[
                        b * capp : b * capp + cap
                    ].astype(BF16)

            loop(T, piece)

        @pl.when(q == n - 1)
        def _():
            loop(n - 3, lambda k: give_chunk(k + 1))

        @pl.when(last)
        def _():
            give_chunk(n - 1)
            give_chunk(0)

    loop(n + 1, step)

    hid_t[...] = hid[...].T
    gback_t[...] = gback[...].T
    uback_t[...] = uback[...].T
    jobs = ((hid_t, 1, ddown_ref), (gback_t, 0, dgate_ref), (uback_t, 0, dup_ref))
    width = 512
    tiles = T * d // width

    def weight_piece(k):
        for which, (left, i, out) in enumerate(jobs):

            @pl.when(k // tiles == which)
            def _(left=left, i=i, out=out):
                at = pl.ds(pl.multiple_of(lax.rem(k, tiles) * width, width), width)
                out[:, at] = jnp.dot(
                    left[...], xc[i, :, at], preferred_element_type=F32
                ).astype(BF16)

    steps = S + lag + 1 - 4
    each = -(-3 * tiles // (steps - 1))

    def finish_step(t):
        for k in range(each):

            @pl.when(t * each + k < 3 * tiles)
            def _(k=k):
                weight_piece(t * each + k)

        service(t + 4)

    loop(steps, finish_step)

    total_ref[...] = gin_ref[...].astype(F32)

    def gathered(r):
        j = block(r)
        at = dest(j)

        @pl.when(j != 0)
        def _():
            zback(j, True).wait_recv()

        chosen = (slots == code_ref[pl.ds(at, 1), :]).astype(F32).astype(BF16)
        total_ref[...] += contract_first(chosen, back[at])

    loop(S, gathered)
    value = total_ref[...].astype(BF16)
    own_ref[...] = value
    full_ref[:, cols(p)] = value

    def acopy(r, arriving=False):
        at = lax.rem(p - r + T, T) if arriving else p
        return remote(
            own_ref, full_ref.at[:, cols(at)], asend.at[r - 1], arecv.at[r - 1],
            tp=lax.rem(p + r, T),
        )

    loop(S - 1, lambda k: zback(k + 1).wait_send())
    for r in range(1, T):
        acopy(r).start()

    def drain(j):
        for i in range(2):

            @pl.when(j > 0)
            def _(i=i):
                zcopy(i, j).wait_send()

            for k in range(len(partners)):
                fcopy(i, j, k).wait_send()
                if relay:
                    rcopy(i, j, k).wait_send()
        if relay:
            for h in range(2):
                tcopy(j, h, 0).wait_send()
                tcopy(j, h, 1).wait_send()
                bcopy(j, h).wait_send()
        else:
            for r in range(1, T):
                tcopy(j, r).wait_send()

    loop(S, drain)
    for k in range(2):
        hcopy(k).wait()
    for r in range(1, T):
        acopy(r).wait_send()
        acopy(r, True).wait_recv()


def finish_kernel(
    dgate, dup, ddown, own_ref, sum_ref, dgate_out, dup_out, ddown_out, own_out, sum_out, sem
):
    copies = [
        pltpu.make_async_copy(src, dst, sem.at[i])
        for i, (src, dst) in enumerate(((dgate, dgate_out), (dup, dup_out), (ddown, ddown_out)))
    ]
    for copy in copies:
        copy.start()
    own_out[...] = own_ref[...]
    sum_out[...] = sum_ref[...]
    for copy in copies:
        copy.wait()


def reduce_kernel(
    S, proj_ref, edge_ref, sum_ref, halo_ref,
    given, pairs, landed, gsend, grecv, psend, precv, hsend, hrecv,
):
    s = lax.axis_index("sp")
    n = S // 2
    z, c = s // 2, lax.rem(s, 2)
    enter((("sp", S),))()

    def hcopy(k):
        to = lax.rem(s + (1 if k == 0 else S - 1), S)
        return remote(
            edge_ref.at[1 - k], halo_ref.at[k], hsend.at[k], hrecv.at[k], sp=to
        )

    def at(o):
        return lax.rem(z + o, n)

    def gcopy(o):
        return remote(
            proj_ref.at[2 * at(o) + 1 - c], given.at[at(o)],
            gsend.at[o], grecv.at[o], sp=s + 1 - 2 * c,
        )

    def pcopy(o):
        return remote(
            pairs.at[at(o)], landed.at[o - 1], psend.at[o - 1], precv.at[o - 1],
            sp=2 * at(o) + c,
        )

    for k in range(2):
        hcopy(k).start()
    for o in range(1, n + 1):
        gcopy(o % n).start()

    def pair(o):
        gcopy(o).wait_recv()
        return proj_ref[2 * at(o) + c].astype(F32) + given[at(o)].astype(F32)

    for o in range(1, n):
        pairs[at(o)] = pair(o).astype(BF16)
        if o > 1:
            pcopy(o - 1).start()
    sum_ref[...] = pair(0)
    pcopy(n - 1).start()
    for o in range(1, n):
        pcopy(o).wait_recv()
        sum_ref[...] += landed[o - 1].astype(F32)
    for o in range(n):
        gcopy(o).wait_send()
        if o > 0:
            pcopy(o).wait_send()
    for k in range(2):
        hcopy(k).wait()


def vmem(count):
    return [pl.BlockSpec(memory_space=pltpu.VMEM)] * count


def params(number):
    return pltpu.CompilerParams(
        collective_id=number, has_side_effects=True, vmem_limit_bytes=16 * 2**20
    )


def rimmed(value, halo):
    s, size = lax.axis_index("sp"), lax.axis_size("sp")
    before = jnp.where(s > 0, halo[0, -1:], 0.0)
    after = jnp.where(s < size - 1, halo[1, :1], 0.0)
    return jnp.concatenate([before, value, after], axis=0)


def edges(value):
    return jnp.stack([value[:8], value[-8:]])


def body(
    routes, route_weights, expert_inputs, out_grad, w_gate, w_up, w_down,
    conv_u, conv_b, conv_c, conv_taps, out_proj,
):
    S, T = lax.axis_size("sp"), lax.axis_size("tp")
    tokens, d = expert_inputs.shape
    channels = conv_u.shape[1]
    cap = 3 * tokens // S
    capp = padded_rows(cap)
    hidden = w_gate.shape[1]
    dma = pltpu.SemaphoreType.DMA
    ways = 2 if T == 4 else T - 1
    relays = (2, S, 2) if T == 4 else (1, 1, 1)
    if T == 4:
        pieces = 4
        shapes = ((2, 2, S, cap, d // 2), (2, S, cap, d // 2), (2, S, cap, d // 2))
    else:
        pieces = T - 1
        shapes = ((T - 1, S, cap, d), (8, 128), (8, 128))
    landing = [pltpu.VMEM(shape, BF16) for shape in shapes]
    mixed_in = conv_c.astype(F32) * conv_u.astype(F32)
    halo_shape = jax.ShapeDtypeStruct((2, 8, channels), F32)
    grad_w = jax.ShapeDtypeStruct((hidden, T * d), BF16)
    anywhere = pl.BlockSpec(memory_space=pl.ANY)
    grad_input, grad_full, halo, grad_gate, grad_up, grad_down = pl.pallas_call(
        functools.partial(expert_kernel, S, T),
        out_shape=(
            jax.ShapeDtypeStruct((tokens, d), BF16),
            jax.ShapeDtypeStruct((tokens, T * d), BF16),
            halo_shape,
            grad_w,
            grad_w,
            grad_w,
        ),
        in_specs=vmem(5) + [anywhere] * 3,
        out_specs=tuple(vmem(6)),
        scratch_shapes=[
            pltpu.VMEM((hidden, T * d), BF16),
            pltpu.VMEM((hidden, T * d), BF16),
            pltpu.VMEM((hidden, T * d), BF16),
            pltpu.VMEM((S, tokens), jnp.int32),
            pltpu.VMEM((S, tokens), F32),
            pltpu.VMEM((2, S, cap, d), BF16),
            pltpu.VMEM((2, S, cap, T * d), BF16),
            pltpu.VMEM((2, S * capp, T * d), BF16),
            pltpu.VMEM((2 * capp, hidden), F32),
            pltpu.VMEM((2 * capp, hidden), F32),
            pltpu.VMEM((S * capp, hidden), BF16),
            pltpu.VMEM((S * capp, hidden), BF16),
            pltpu.VMEM((S * capp, hidden), BF16),
            pltpu.VMEM((hidden, S * capp), BF16),
            pltpu.VMEM((hidden, S * capp), BF16),
            pltpu.VMEM((hidden, S * capp), BF16),
            pltpu.VMEM((S, cap, T * d), BF16),
            *landing,
            pltpu.VMEM((S, cap, d), BF16),
            pltpu.VMEM((S, cap, d), BF16),
            pltpu.VMEM((tokens, d), F32),
            dma((3,)),
            dma((2, S)),
            dma((2, S)),
            dma((2, S, ways)),
            dma((2, S, ways)),
            dma(relays),
            dma(relays),
            dma((S, pieces)),
            dma((S, pieces)),
            dma(relays[1:]),
            dma(relays[1:]),
            dma((S,)),
            dma((S,)),
            dma((T - 1,)),
            dma((T - 1,)),
            dma((2,)),
            dma((2,)),
        ],
        compiler_params=pltpu.CompilerParams(
            collective_id=0, has_side_effects=True, vmem_limit_bytes=56 * 2**20
        ),
        name="experts",
    )(
        routes.T, route_weights.T, expert_inputs, out_grad, edges(mixed_in),
        w_gate, w_up, w_down,
    )

    padded = rimmed(mixed_in, halo)
    convolved = (
        conv_taps[0] * padded[0:tokens]
        + conv_taps[1] * padded[1 : tokens + 1]
        + conv_taps[2] * padded[2 : tokens + 2]
    )
    conv_out = (conv_b.astype(F32) * convolved).astype(BF16)
    grad_conv = contract_last(grad_full, out_proj)
    grad_b = (grad_conv * convolved).astype(BF16)
    grad_mixed = grad_conv * conv_b.astype(F32)
    proj = contract_first(grad_full, conv_out).astype(BF16)
    width = proj.shape[0] // S
    proj_sum, halo = pl.pallas_call(
        functools.partial(reduce_kernel, S),
        out_shape=(jax.ShapeDtypeStruct((width, channels), F32), halo_shape),
        in_specs=vmem(2),
        out_specs=tuple(vmem(2)),
        scratch_shapes=[
            pltpu.VMEM((S // 2, width, channels), BF16),
            pltpu.VMEM((S // 2, width, channels), BF16),
            pltpu.VMEM((S // 2 - 1, width, channels), BF16),
            dma((S // 2,)),
            dma((S // 2,)),
            dma((S // 2 - 1,)),
            dma((S // 2 - 1,)),
            dma((2,)),
            dma((2,)),
        ],
        compiler_params=params(2),
        name="sum_proj",
    )(proj.reshape(S, width, channels), edges(grad_mixed))
    rim = rimmed(grad_mixed, halo)
    grad_z = (
        conv_taps[0] * rim[2 : tokens + 2]
        + conv_taps[1] * rim[1 : tokens + 1]
        + conv_taps[2] * rim[0:tokens]
    )
    grad_c = (grad_z * conv_u.astype(F32)).astype(BF16)
    grad_u = (grad_z * conv_c.astype(F32)).astype(BF16)
    grad_gate, grad_up, grad_down, grad_input, proj_sum = pl.pallas_call(
        finish_kernel,
        out_shape=tuple(
            jax.ShapeDtypeStruct(v.shape, v.dtype)
            for v in (grad_gate, grad_up, grad_down, grad_input, proj_sum)
        ),
        in_specs=vmem(5),
        out_specs=tuple([anywhere] * 3 + vmem(2)),
        scratch_shapes=[dma((3,))],
        compiler_params=pltpu.CompilerParams(vmem_limit_bytes=32 * 2**20),
        name="finish",
    )(grad_gate, grad_up, grad_down, grad_input, proj_sum)
    return (
        grad_gate[None], grad_up[None], grad_down[None], grad_input, proj_sum,
        grad_u, grad_b, grad_c,
    )


def solution(mesh):
    in_specs = (
        P("sp", None),
        P("sp", None),
        P("sp", "tp"),
        P("sp", "tp"),
        P("sp", "tp", None),
        P("sp", "tp", None),
        P("sp", "tp", None),
        P("sp", "tp"),
        P("sp", "tp"),
        P("sp", "tp"),
        P(None, "tp"),
        P("tp", None),
    )
    out_specs = (
        P("sp", "tp", None),
        P("sp", "tp", None),
        P("sp", "tp", None),
        P("sp", "tp"),
        P("sp", "tp"),
        P("sp", "tp"),
        P("sp", "tp"),
        P("sp", "tp"),
    )
    return jax.shard_map(body, mesh=mesh, in_specs=in_specs, out_specs=out_specs, check_vma=False)
```

time: 155 us -> 118 us (0.76)
  matrix products: 30.7 us -> 3.76 us
  Pallas kernels: 113 us -> 106 us
    dot_general x4 -> x1, matrix products: 14.8 us -> 1.63 us  [contract_first(): lax.dot_general(left, right, (((0,), (0,)), ((), ())), preferred_element_...]
    dot_general x4 -> x1, matrix products: 10.5 us -> 2.12 us  [contract_last(): lax.dot_general(left, right, (((1,), (1,)), ((), ())), preferred_element_...]
    dot_general x2 -> x0, matrix products: 5.44 us -> none  [the longest x1 3.44 us: body(): jnp.dot(up_back, up_weight, preferred_element_type=F32)]
    pallas_call x1, Pallas kernels: 14.4 us -> 10.1 us  [body(): pl.pallas_call(functools.partial(reduce_kernel, S), out_shape=(jax.ShapeD...]
    pallas_call x2, Pallas kernels: 98.8 us -> 95.9 us  [the longest x1 91.7 us: body(): pl.pallas_call(functools.partial(expert_kernel, S, T), out_shape=(jax.Sha...]
    unnamed x28 -> x16, local copies, waits for them, and re-layouts: 4.36 us -> 3.66 us
where the time goes in v1:
time: 118 us
  Pallas kernels  106 us (90%)
  local copies, waits for them, and re-layouts  4.47 us (4%)
  matrix products  3.76 us (3%)
  other arithmetic  3.05 us (3%)
    pallas_call x1, Pallas kernels, body(): pl.pallas_call(functools.partial(expert_kernel, S, T), out_shape=(jax.Sha...  91.7 us
    pallas_call x1, Pallas kernels, body(): pl.pallas_call(functools.partial(reduce_kernel, S), out_shape=(jax.ShapeD...  10.1 us
    pallas_call x1, Pallas kernels, body(): pl.pallas_call(finish_kernel, out_shape=tuple((jax.ShapeDtypeStruct(v.sha...  4.22 us
    unnamed x16, local copies, waits for them, and re-layouts  3.66 us

profile of v1, /device:TPU:0, one launch (start us, length us, event | category | flops | bytes accessed | tf_op | source)
XLA Modules:
  0.0 117.9 jit_solution(18194281087349853510)
XLA Ops:
  0.6 0.0 copy-start
  0.6 0.9 convert_multiply_fusion.3
  1.6 0.6 pad_maximum_fusion.4.edge_ref
  2.2 0.0 copy-start.5
  2.2 91.7 %experts.1 = (bf16[192,512]{1,0:T(8,128)(2,1)}, bf16[192,2048]{1,0:T(8,128)(2,1)}, f32[2,8,128]{2,1,0:T(8,128)}, bf16[704,2048]{1,0:T(8,128)(2,1)}, bf16[704,204...) custom-call(s32[2,192]{1,0:T(2,128)} %bitcast.32, f32[2,192]{1,0:T(2,128)} %bitcast.33, bf16[192,512]{1,0:T(8,128)(2,1)} %xin_ref.1, ...), custom_call_target="tpu_custom_call" | custom-call | tf_op jit(solution)/shard_map/experts/pallas_call | solution.py:617
  93.8 0.0 copy-start.1
  93.8 0.0 copy-start.6
  93.9 0.0 copy-start.7
  93.9 0.0 copy-start.4
  93.9 0.8 fusion.13
  94.7 0.8 slice_bitcast_fusion.6
  95.5 0.0 copy-done
  95.5 0.0 copy-done.5
  95.5 2.1 %multiply_convert_fusion = (bf16[192,128]{1,0:T(8,128)(2,1)}, f32[192,128]{1,0:T(8,128)S(1)}) fusion(f32[1,128]{1,0:T(1,128)S(1)} %get-tuple-element.45, f32[192,128]{1,0:T(8,128)S(1)} %convert_multiply_fusion.3, f32[128]{0:T(128)S(1)} %get-tuple-element.47, f32[128]{0:T(128)S(1)} %get-tuple-element.48, f32[1,128]{1,0:T(1,128)S(1)} %get-tuple-element.44, ...), kind=kOutput, calls=%fused_computation.21 | convolution fusion | flops 100933632 | bytes 1608192 | tf_op jit(solution)/shard_map/dot_general | solution.py:22
  97.7 1.6 %convolution_convert_fusion = bf16[2048,128]{1,0:T(8,128)(2,1)S(1)} fusion(bf16[192,2048]{1,0:T(8,128)(2,1)} %get-tuple-element.25, bf16[192,128]{1,0:T(8,128)(2,1)S(1)} %copy-done.5, f32[1,128]{1,0:T(1,128)S(1)} %get-tuple-element.45, f32[192,128]{1,0:T(8,128)S(1)} %convert_multiply_fusion.3, f32[1,128]{1,0:T(1,128)S(1)} %get-tuple-element.44, ...), kind=kOutput, calls=%fused_computation | convolution fusion | flops 101171200 | bytes 1460736 | tf_op jit(solution)/shard_map/dot_general | solution.py:16
  99.3 10.1 %sum_proj.1 = (f32[256,128]{1,0:T(8,128)S(1)}, f32[2,8,128]{2,1,0:T(8,128)S(1)}) custom-call(bf16[8,256,128]{2,1,0:T(8,128)(2,1)S(1)} %bitcast.31, f32[2,8,128]{2,1,0:T(8,128)S(1)} %pad_maximum_fusion.5.edge_ref), custom_call_target="tpu_custom_call" | custom-call | tf_op jit(solution)/shard_map/sum_proj/pallas_call | solution.py:690
  109.4 0.0 copy-done.6
  109.4 0.0 copy-done.7
  109.4 0.7 fusion.1
  110.1 0.0 copy-done.1
  110.1 0.0 copy-done.4
  110.1 0.0 copy-start.2
  110.1 1.8 %copy-done.2 = bf16[704,2048]{1,0:T(8,128)(2,1)S(1)} copy-done((bf16[704,2048]{1,0:T(8,128)(2,1)S(1)}, bf16[704,2048]{1,0:T(8,128)(2,1)}, u32[]{:S(2)}) %copy-start.2) | copy-done | bytes 2883608
  111.9 0.0 copy-start.3
  111.9 1.8 %copy-done.3 = bf16[704,2048]{1,0:T(8,128)(2,1)S(1)} copy-done((bf16[704,2048]{1,0:T(8,128)(2,1)S(1)}, bf16[704,2048]{1,0:T(8,128)(2,1)}, u32[]{:S(2)}) %copy-start.3) | copy-done | bytes 2883608
  113.7 4.2 %finish.1 = (bf16[704,2048]{1,0:T(8,128)(2,1)}, bf16[704,2048]{1,0:T(8,128)(2,1)}, bf16[704,2048]{1,0:T(8,128)(2,1)}, bf16[192,512]{1,0:T(8,128)(2,1)}, f32[256,128]{1,0:T(8,128)}) custom-call(bf16[704,2048]{1,0:T(8,128)(2,1)S(1)} %copy-done.1, bf16[704,2048]{1,0:T(8,128)(2,1)S(1)} %copy-done.2, bf16[704,2048]{1,0:T(8,128)(2,1)S(1)} %copy-done.3, ...), custom_call_target="tpu_custom_call" | custom-call | tf_op jit(solution)/shard_map/finish/pallas_call | solution.py:717
  (4 shorter events, 0.0 us)
Async XLA Ops:
  0.6 94.9 %copy-start = (bf16[128,2048]{1,0:T(8,128)(2,1)S(1)}, bf16[128,2048]{1,0:T(8,128)(2,1)}, u32[]{:S(2)}) copy-start(bf16[128,2048]{1,0:T(8,128)(2,1)} %param.23) | copy-start | bytes 1572868
  2.2 93.4 %copy-start.5 = (bf16[192,128]{1,0:T(8,128)(2,1)S(1)}, bf16[192,128]{1,0:T(8,128)(2,1)}, u32[]{:S(2)}) copy-start(bf16[192,128]{1,0:T(8,128)(2,1)} %param.20) | copy-start | bytes 147460
  93.8 16.3 %copy-start.1 = (bf16[704,2048]{1,0:T(8,128)(2,1)S(1)}, bf16[704,2048]{1,0:T(8,128)(2,1)}, u32[]{:S(2)}) copy-start(bf16[704,2048]{1,0:T(8,128)(2,1)} %get-tuple-element.21.dgate) | copy-start | bytes 8650756
  93.8 15.5 %copy-start.6 = (bf16[192,128]{1,0:T(8,128)(2,1)S(1)}, bf16[192,128]{1,0:T(8,128)(2,1)}, u32[]{:S(2)}) copy-start(bf16[192,128]{1,0:T(8,128)(2,1)} %param.19) | copy-start | bytes 147460
  93.9 15.5 %copy-start.7 = (bf16[192,128]{1,0:T(8,128)(2,1)S(1)}, bf16[192,128]{1,0:T(8,128)(2,1)}, u32[]{:S(2)}) copy-start(bf16[192,128]{1,0:T(8,128)(2,1)} %param.21) | copy-start | bytes 147460
  93.9 16.2 %copy-start.4 = (bf16[192,512]{1,0:T(8,128)(2,1)S(1)}, bf16[192,512]{1,0:T(8,128)(2,1)}, u32[]{:S(2)}) copy-start(bf16[192,512]{1,0:T(8,128)(2,1)} %get-tuple-element.24.own_ref) | copy-start | bytes 589828
  110.1 1.8 %copy-start.2 = (bf16[704,2048]{1,0:T(8,128)(2,1)S(1)}, bf16[704,2048]{1,0:T(8,128)(2,1)}, u32[]{:S(2)}) copy-start(bf16[704,2048]{1,0:T(8,128)(2,1)} %get-tuple-element.22.dup) | copy-start | bytes 8650756
  111.9 1.8 %copy-start.3 = (bf16[704,2048]{1,0:T(8,128)(2,1)S(1)}, bf16[704,2048]{1,0:T(8,128)(2,1)}, u32[]{:S(2)}) copy-start(bf16[704,2048]{1,0:T(8,128)(2,1)} %get-tuple-element.23.ddown) | copy-start | bytes 8650756

commit v2 on v1

--- a/solution.py
+++ b/solution.py
@@ -74,28 +74,43 @@
 
 
 def expert_kernel(
-    S, T, routes_ref, wts_ref, xin_ref, gin_ref, edge_ref, gate_hbm, up_hbm, down_hbm,
-    own_ref, full_ref, halo_ref, dgate_ref, dup_ref, ddown_ref,
-    gate_w, up_w, down_w, code_ref, weight_ref, zs, xg, xc, pre, upre,
+    S, T, routes_hbm, wts_hbm, xin_hbm, gin_hbm, gate_hbm, up_hbm, down_hbm,
+    u_hbm, b_hbm, c_hbm, taps_hbm, outw_hbm,
+    own_ref, sum_ref, gu_ref, gb_ref, gc_ref, dgate_ref, dup_ref, ddown_ref,
+    routes_ref, wts_ref, xin_ref, gin_ref, gate_w, up_w, down_w,
+    u_ref, b_ref, c_ref, taps_ref, out_w,
+    code_ref, weight_ref, zs, xg, xc, pre, upre,
     hid, gback, uback, hid_t, gback_t, uback_t, part, landed, met, passed, summed, back, total_ref,
-    wsem, zsend, zrecv, fsend, frecv, rsend, rrecv,
+    full_ref, edge_ref, halo_ref, rim, conv_ref, y_ref, dy_ref, proj, given, pairs, arrived,
+    isem, zsend, zrecv, fsend, frecv, rsend, rrecv,
     tsend, trecv, bsend, brecv, ysend, yrecv, asend, arecv, hsend, hrecv,
+    gsend, grecv, psend, precv,
 ):
     s, p = lax.axis_index("sp"), lax.axis_index("tp")
     n = S // 2
     z, c = s // 2, lax.rem(s, 2)
     cap, d = summed.shape[1], summed.shape[2]
+    tokens = own_ref.shape[0]
     capp = padded_rows(cap)
     half = d // 2
     relay = T == 4
     wait_entry = enter((("sp", S), ("tp", T)))
 
-    weights = [
-        pltpu.make_async_copy(src.at[0], dst, wsem.at[i])
-        for i, (src, dst) in enumerate(((gate_hbm, gate_w), (up_hbm, up_w), (down_hbm, down_w)))
+    loads = [
+        pltpu.make_async_copy(src, dst, isem.at[i])
+        for i, (src, dst) in enumerate(
+            (
+                (routes_hbm, routes_ref), (wts_hbm, wts_ref), (xin_hbm, xin_ref),
+                (gin_hbm, gin_ref), (u_hbm, u_ref), (c_hbm, c_ref), (gate_hbm.at[0], gate_w),
+                (up_hbm.at[0], up_w), (down_hbm.at[0], down_w), (b_hbm, b_ref),
+                (taps_hbm, taps_ref), (outw_hbm, out_w),
+            )
+        )
     ]
-    for w in weights:
-        w.start()
+    for load in loads:
+        load.start()
+    for load in loads[:4]:
+        load.wait()
 
     def offset(q):
         odd = lax.rem(q, 2)
@@ -298,14 +313,45 @@
 
     loop(S - 1, send_picked)
 
-    def hcopy(k):
+    def hcopy(turn, k):
         to = lax.rem(s + (1 if k == 0 else S - 1), S)
         return remote(
-            edge_ref.at[1 - k], halo_ref.at[k], hsend.at[k], hrecv.at[k], sp=to
+            edge_ref.at[turn, 1 - k], halo_ref.at[turn, k],
+            hsend.at[turn, k], hrecv.at[turn, k], sp=to,
         )
 
-    for k in range(2):
-        hcopy(k).start()
+    sends = (s < S - 1, s > 0)
+    takes = (s > 0, s < S - 1)
+
+    def greet_edges(turn, value):
+        edge_ref[turn, 0] = value[:8]
+        edge_ref[turn, 1] = value[tokens - 8 :]
+
+    def send_edges(turn):
+        for k in range(2):
+
+            @pl.when(sends[k])
+            def _(k=k):
+                hcopy(turn, k).start()
+
+    def take_edges(turn, value):
+        rim[8 : 8 + tokens] = value
+        rim[0:8] = jnp.zeros_like(rim[0:8])
+        rim[8 + tokens : 16 + tokens] = jnp.zeros_like(rim[0:8])
+        for k in range(2):
+
+            @pl.when(takes[k])
+            def _(k=k):
+                hcopy(turn, k).wait_recv()
+                at = (0, 8 + tokens)[k]
+                rim[at : at + 8] = halo_ref[turn, k]
+
+    def mixed_in():
+        return c_ref[...].astype(F32) * u_ref[...].astype(F32)
+
+    for load in loads[4:6]:
+        load.wait()
+    greet_edges(0, mixed_in())
 
     def chunk(q):
         return pl.ds(pl.multiple_of(q * 2 * capp, 2 * capp), 2 * capp)
@@ -332,8 +378,8 @@
 
             @pl.when(q == 1)
             def _():
-                for w in weights:
-                    w.wait()
+                for load in loads[6:9]:
+                    load.wait()
 
             pre[...] = contract_last(xc[0, chunk(q - 1), :], gate_w[...])
 
@@ -408,7 +454,20 @@
             give_chunk(n - 1)
             give_chunk(0)
 
+    send_edges(0)
     loop(n + 1, step)
+
+    for load in loads[9:]:
+        load.wait()
+    take_edges(0, mixed_in())
+    taps = [taps_ref[i : i + 1, :] for i in range(3)]
+    convolved = (
+        taps[0] * rim[7 : 7 + tokens]
+        + taps[1] * rim[8 : 8 + tokens]
+        + taps[2] * rim[9 : 9 + tokens]
+    )
+    conv_ref[...] = convolved
+    y_ref[...] = (b_ref[...].astype(F32) * convolved).astype(BF16)
 
     hid_t[...] = hid[...].T
     gback_t[...] = gback[...].T
@@ -458,17 +517,131 @@
     value = total_ref[...].astype(BF16)
     own_ref[...] = value
     full_ref[:, cols(p)] = value
-
-    def acopy(r, arriving=False):
-        at = lax.rem(p - r + T, T) if arriving else p
+    dy_ref[...] = jnp.zeros_like(dy_ref)
+    width = proj.shape[1]
+
+    if relay:
+
+        def acopy(k, h, arriving=False):
+            to = (xn, yn)[k]
+            view = full_ref.at[:, halfcols(to if arriving else p, h)]
+            return remote(view, view, asend.at[2 * k + h], arecv.at[2 * k + h], tp=to)
+
+        def arelay(k, arriving=False):
+            near, far = ((xn, yn), (yn, xn))[k]
+            view = full_ref.at[:, halfcols(3 - p if arriving else near, k)]
+            return remote(view, view, asend.at[4 + k], arecv.at[4 + k], tp=far)
+
+        for h in range(2):
+            acopy(0, h).start()
+            acopy(1, 1 - h).start()
+
+        def hand_on():
+            for k in range(2):
+                acopy(k, k, True).wait_recv()
+                arelay(k).start()
+
+        def near_piece(k):
+            acopy(k, 1 - k, True).wait_recv()
+
+        def far_piece():
+            for k in range(2):
+                arelay(k, True).wait_recv()
+
+        order_in = (
+            (p, hand_on),
+            (xn, lambda: near_piece(0)),
+            (yn, lambda: near_piece(1)),
+            (3 - p, far_piece),
+        )
+        gathers = [acopy(k, h) for k in range(2) for h in range(2)] + [arelay(0), arelay(1)]
+    else:
+
+        def acopy(r, arriving=False):
+            at = lax.rem(p - r + T, T) if arriving else p
+            view = full_ref.at[:, cols(at)]
+            return remote(
+                view, view, asend.at[r - 1], arecv.at[r - 1], tp=lax.rem(p + r, T)
+            )
+
+        for r in range(1, T):
+            acopy(r).start()
+        order_in = ((p, lambda: None),) + tuple(
+            (lax.rem(p - r + T, T), lambda r=r: acopy(r, True).wait_recv())
+            for r in range(1, T)
+        )
+        gathers = [acopy(r) for r in range(1, T)]
+
+    def gcopy(q):
         return remote(
-            own_ref, full_ref.at[:, cols(at)], asend.at[r - 1], arecv.at[r - 1],
-            tp=lax.rem(p + r, T),
+            proj.at[2 * q + 1 - c], given.at[q], gsend.at[q], grecv.at[q], sp=s + 1 - 2 * c
         )
 
-    loop(S - 1, lambda k: zback(k + 1).wait_send())
-    for r in range(1, T):
-        acopy(r).start()
+    def pcopy(q):
+        return remote(pairs.at[q], arrived.at[z], psend.at[q], precv.at[z], sp=2 * q + c)
+
+    def pcopy_in(q):
+        return remote(pairs.at[q], arrived.at[q], psend.at[q], precv.at[q], sp=2 * q + c)
+
+    def mix(q):
+        piece = full_ref[:, cols(q)]
+        dy_ref[...] += contract_last(piece, out_w[:, cols(q)])
+        value = contract_first(piece, y_ref[...]).astype(BF16)
+        proj[2 * q] = value[:width]
+        proj[2 * q + 1] = value[width:]
+
+    def pair(q):
+        gcopy(q).wait_recv()
+        both = proj[2 * q + c].astype(F32) + given[q].astype(F32)
+
+        @pl.when(q == z)
+        def _():
+            sum_ref[...] = both
+
+        @pl.when(q != z)
+        def _():
+            pairs[q] = both.astype(BF16)
+
+    def post(q):
+        @pl.when(q != z)
+        def _():
+            pcopy(q).start()
+
+    for k, (q, arrive) in enumerate(order_in):
+        if k == 0:
+            mix(q)
+            arrive()
+            gcopy(q).start()
+            continue
+        arrive()
+        mix(q)
+        pair(order_in[k - 1][0])
+        gcopy(q).start()
+        post(order_in[k - 1][0])
+    last_piece = order_in[-1][0]
+    grad_mixed = dy_ref[...] * b_ref[...].astype(F32)
+    greet_edges(1, grad_mixed)
+    gb_ref[...] = (dy_ref[...] * conv_ref[...]).astype(BF16)
+    pair(last_piece)
+    send_edges(1)
+    post(last_piece)
+    take_edges(1, grad_mixed)
+    grad_z = (
+        taps[0] * rim[9 : 9 + tokens]
+        + taps[1] * rim[8 : 8 + tokens]
+        + taps[2] * rim[7 : 7 + tokens]
+    )
+    gc_ref[...] = (grad_z * u_ref[...].astype(F32)).astype(BF16)
+    gu_ref[...] = (grad_z * c_ref[...].astype(F32)).astype(BF16)
+
+    def collect(q):
+        @pl.when(q != z)
+        def _():
+            pcopy_in(q).wait_recv()
+            sum_ref[...] += arrived[q].astype(F32)
+            pcopy(q).wait_send()
+
+        gcopy(q).wait_send()
 
     def drain(j):
         for i in range(2):
@@ -491,103 +664,32 @@
                 tcopy(j, r).wait_send()
 
     loop(S, drain)
-    for k in range(2):
-        hcopy(k).wait()
-    for r in range(1, T):
-        acopy(r).wait_send()
-        acopy(r, True).wait_recv()
-
-
-def finish_kernel(
-    dgate, dup, ddown, own_ref, sum_ref, dgate_out, dup_out, ddown_out, own_out, sum_out, sem
-):
+    loop(S - 1, lambda k: zback(k + 1).wait_send())
+    for gather in gathers:
+        gather.wait_send()
+    for turn in range(2):
+        for k in range(2):
+
+            @pl.when(sends[k])
+            def _(turn=turn, k=k):
+                hcopy(turn, k).wait_send()
+
+    loop(n, collect)
+
+
+def finish_kernel(count, *refs):
+    sem = refs[2 * count]
     copies = [
-        pltpu.make_async_copy(src, dst, sem.at[i])
-        for i, (src, dst) in enumerate(((dgate, dgate_out), (dup, dup_out), (ddown, ddown_out)))
+        pltpu.make_async_copy(refs[i], refs[count + i], sem.at[i]) for i in range(count)
     ]
     for copy in copies:
         copy.start()
-    own_out[...] = own_ref[...]
-    sum_out[...] = sum_ref[...]
     for copy in copies:
         copy.wait()
 
 
-def reduce_kernel(
-    S, proj_ref, edge_ref, sum_ref, halo_ref,
-    given, pairs, landed, gsend, grecv, psend, precv, hsend, hrecv,
-):
-    s = lax.axis_index("sp")
-    n = S // 2
-    z, c = s // 2, lax.rem(s, 2)
-    enter((("sp", S),))()
-
-    def hcopy(k):
-        to = lax.rem(s + (1 if k == 0 else S - 1), S)
-        return remote(
-            edge_ref.at[1 - k], halo_ref.at[k], hsend.at[k], hrecv.at[k], sp=to
-        )
-
-    def at(o):
-        return lax.rem(z + o, n)
-
-    def gcopy(o):
-        return remote(
-            proj_ref.at[2 * at(o) + 1 - c], given.at[at(o)],
-            gsend.at[o], grecv.at[o], sp=s + 1 - 2 * c,
-        )
-
-    def pcopy(o):
-        return remote(
-            pairs.at[at(o)], landed.at[o - 1], psend.at[o - 1], precv.at[o - 1],
-            sp=2 * at(o) + c,
-        )
-
-    for k in range(2):
-        hcopy(k).start()
-    for o in range(1, n + 1):
-        gcopy(o % n).start()
-
-    def pair(o):
-        gcopy(o).wait_recv()
-        return proj_ref[2 * at(o) + c].astype(F32) + given[at(o)].astype(F32)
-
-    for o in range(1, n):
-        pairs[at(o)] = pair(o).astype(BF16)
-        if o > 1:
-            pcopy(o - 1).start()
-    sum_ref[...] = pair(0)
-    pcopy(n - 1).start()
-    for o in range(1, n):
-        pcopy(o).wait_recv()
-        sum_ref[...] += landed[o - 1].astype(F32)
-    for o in range(n):
-        gcopy(o).wait_send()
-        if o > 0:
-            pcopy(o).wait_send()
-    for k in range(2):
-        hcopy(k).wait()
-
-
 def vmem(count):
     return [pl.BlockSpec(memory_space=pltpu.VMEM)] * count
-
-
-def params(number):
-    return pltpu.CompilerParams(
-        collective_id=number, has_side_effects=True, vmem_limit_bytes=16 * 2**20
-    )
-
-
-def rimmed(value, halo):
-    s, size = lax.axis_index("sp"), lax.axis_size("sp")
-    before = jnp.where(s > 0, halo[0, -1:], 0.0)
-    after = jnp.where(s < size - 1, halo[1, :1], 0.0)
-    return jnp.concatenate([before, value, after], axis=0)
-
-
-def edges(value):
-    return jnp.stack([value[:8], value[-8:]])
 
 
 def body(
@@ -610,26 +712,36 @@
         pieces = T - 1
         shapes = ((T - 1, S, cap, d), (8, 128), (8, 128))
     landing = [pltpu.VMEM(shape, BF16) for shape in shapes]
-    mixed_in = conv_c.astype(F32) * conv_u.astype(F32)
-    halo_shape = jax.ShapeDtypeStruct((2, 8, channels), F32)
-    grad_w = jax.ShapeDtypeStruct((hidden, T * d), BF16)
+    width = T * d // S
+    outs = (
+        pltpu.VMEM((tokens, d), BF16),
+        pltpu.VMEM((width, channels), F32),
+        pltpu.VMEM((tokens, channels), BF16),
+        pltpu.VMEM((tokens, channels), BF16),
+        pltpu.VMEM((tokens, channels), BF16),
+        pltpu.VMEM((hidden, T * d), BF16),
+        pltpu.VMEM((hidden, T * d), BF16),
+        pltpu.VMEM((hidden, T * d), BF16),
+    )
     anywhere = pl.BlockSpec(memory_space=pl.ANY)
-    grad_input, grad_full, halo, grad_gate, grad_up, grad_down = pl.pallas_call(
+    results = pl.pallas_call(
         functools.partial(expert_kernel, S, T),
-        out_shape=(
-            jax.ShapeDtypeStruct((tokens, d), BF16),
-            jax.ShapeDtypeStruct((tokens, T * d), BF16),
-            halo_shape,
-            grad_w,
-            grad_w,
-            grad_w,
-        ),
-        in_specs=vmem(5) + [anywhere] * 3,
-        out_specs=tuple(vmem(6)),
+        out_shape=outs,
+        in_specs=[anywhere] * 12,
+        out_specs=tuple(vmem(8)),
         scratch_shapes=[
+            pltpu.VMEM((2, tokens), jnp.int32),
+            pltpu.VMEM((2, tokens), F32),
+            pltpu.VMEM((tokens, d), BF16),
+            pltpu.VMEM((tokens, d), BF16),
             pltpu.VMEM((hidden, T * d), BF16),
             pltpu.VMEM((hidden, T * d), BF16),
             pltpu.VMEM((hidden, T * d), BF16),
+            pltpu.VMEM((tokens, channels), BF16),
+            pltpu.VMEM((tokens, channels), BF16),
+            pltpu.VMEM((tokens, channels), BF16),
+            pltpu.VMEM((3, channels), F32),
+            pltpu.VMEM((channels, T * d), BF16),
             pltpu.VMEM((S, tokens), jnp.int32),
             pltpu.VMEM((S, tokens), F32),
             pltpu.VMEM((2, S, cap, d), BF16),
@@ -648,7 +760,18 @@
             pltpu.VMEM((S, cap, d), BF16),
             pltpu.VMEM((S, cap, d), BF16),
             pltpu.VMEM((tokens, d), F32),
-            dma((3,)),
+            pltpu.VMEM((tokens, T * d), BF16),
+            pltpu.VMEM((2, 2, 8, channels), F32),
+            pltpu.VMEM((2, 2, 8, channels), F32),
+            pltpu.VMEM((tokens + 16, channels), F32),
+            pltpu.VMEM((tokens, channels), F32),
+            pltpu.VMEM((tokens, channels), BF16),
+            pltpu.VMEM((tokens, channels), F32),
+            pltpu.VMEM((S, width, channels), BF16),
+            pltpu.VMEM((S // 2, width, channels), BF16),
+            pltpu.VMEM((S // 2, width, channels), BF16),
+            pltpu.VMEM((S // 2, width, channels), BF16),
+            dma((12,)),
             dma((2, S)),
             dma((2, S)),
             dma((2, S, ways)),
@@ -661,71 +784,32 @@
             dma(relays[1:]),
             dma((S,)),
             dma((S,)),
-            dma((T - 1,)),
-            dma((T - 1,)),
-            dma((2,)),
-            dma((2,)),
+            dma((6 if T == 4 else T - 1,)),
+            dma((6 if T == 4 else T - 1,)),
+            dma((2, 2)),
+            dma((2, 2)),
+            dma((S // 2,)),
+            dma((S // 2,)),
+            dma((S // 2,)),
+            dma((S // 2,)),
         ],
         compiler_params=pltpu.CompilerParams(
-            collective_id=0, has_side_effects=True, vmem_limit_bytes=56 * 2**20
+            collective_id=0, has_side_effects=True, vmem_limit_bytes=46 * 2**20
         ),
         name="experts",
     )(
-        routes.T, route_weights.T, expert_inputs, out_grad, edges(mixed_in),
-        w_gate, w_up, w_down,
-    )
-
-    padded = rimmed(mixed_in, halo)
-    convolved = (
-        conv_taps[0] * padded[0:tokens]
-        + conv_taps[1] * padded[1 : tokens + 1]
-        + conv_taps[2] * padded[2 : tokens + 2]
-    )
-    conv_out = (conv_b.astype(F32) * convolved).astype(BF16)
-    grad_conv = contract_last(grad_full, out_proj)
-    grad_b = (grad_conv * convolved).astype(BF16)
-    grad_mixed = grad_conv * conv_b.astype(F32)
-    proj = contract_first(grad_full, conv_out).astype(BF16)
-    width = proj.shape[0] // S
-    proj_sum, halo = pl.pallas_call(
-        functools.partial(reduce_kernel, S),
-        out_shape=(jax.ShapeDtypeStruct((width, channels), F32), halo_shape),
-        in_specs=vmem(2),
-        out_specs=tuple(vmem(2)),
-        scratch_shapes=[
-            pltpu.VMEM((S // 2, width, channels), BF16),
-            pltpu.VMEM((S // 2, width, channels), BF16),
-            pltpu.VMEM((S // 2 - 1, width, channels), BF16),
-            dma((S // 2,)),
-            dma((S // 2,)),
-            dma((S // 2 - 1,)),
-            dma((S // 2 - 1,)),
-            dma((2,)),
-            dma((2,)),
-        ],
-        compiler_params=params(2),
-        name="sum_proj",
-    )(proj.reshape(S, width, channels), edges(grad_mixed))
-    rim = rimmed(grad_mixed, halo)
-    grad_z = (
-        conv_taps[0] * rim[2 : tokens + 2]
-        + conv_taps[1] * rim[1 : tokens + 1]
-        + conv_taps[2] * rim[0:tokens]
-    )
-    grad_c = (grad_z * conv_u.astype(F32)).astype(BF16)
-    grad_u = (grad_z * conv_c.astype(F32)).astype(BF16)
-    grad_gate, grad_up, grad_down, grad_input, proj_sum = pl.pallas_call(
-        finish_kernel,
-        out_shape=tuple(
-            jax.ShapeDtypeStruct(v.shape, v.dtype)
-            for v in (grad_gate, grad_up, grad_down, grad_input, proj_sum)
-        ),
-        in_specs=vmem(5),
-        out_specs=tuple([anywhere] * 3 + vmem(2)),
-        scratch_shapes=[dma((3,))],
-        compiler_params=pltpu.CompilerParams(vmem_limit_bytes=32 * 2**20),
+        routes.T, route_weights.T, expert_inputs, out_grad, w_gate, w_up, w_down,
+        conv_u, conv_b, conv_c, conv_taps, out_proj,
+    )
+    grad_input, proj_sum, grad_u, grad_b, grad_c, grad_gate, grad_up, grad_down = pl.pallas_call(
+        functools.partial(finish_kernel, 8),
+        out_shape=tuple(jax.ShapeDtypeStruct(v.shape, v.dtype) for v in outs),
+        in_specs=vmem(8),
+        out_specs=(anywhere,) * 8,
+        scratch_shapes=[dma((8,))],
+        compiler_params=pltpu.CompilerParams(vmem_limit_bytes=8 * 2**20),
         name="finish",
-    )(grad_gate, grad_up, grad_down, grad_input, proj_sum)
+    )(*[pltpu.with_memory_space_constraint(v, pltpu.VMEM) for v in results])
     return (
         grad_gate[None], grad_up[None], grad_down[None], grad_input, proj_sum,
         grad_u, grad_b, grad_c,

time: 118 us -> 95.4 us (0.81); the launches traced: 118 us -> 93.5 us
  Pallas kernels: 106 us -> 92.9 us
  local copies, waits for them, and re-layouts: 4.47 us -> 0 us
  matrix products: 3.76 us -> 0 us
  other arithmetic: 3.05 us -> 0 us
    pallas_call x3 -> x2, Pallas kernels: 106 us -> 92.9 us  [the longest x1 89.2 us: body(): pl.pallas_call(functools.partial(expert_kernel, S, T), out_shape=outs, in...]
    dot_general x2 -> x0, matrix products: 3.76 us -> none  [the longest x1 2.12 us: contract_last(): lax.dot_general(left, right, (((1,), (1,)), ((), ())), preferred_element_...]
    unnamed x16 -> x0, local copies, waits for them, and re-layouts: 3.66 us -> none
where the time goes in v2:
time: 95.4 us; the launch traced here: 93.5 us
  Pallas kernels  92.9 us (97%)
    pallas_call x1, Pallas kernels, body(): pl.pallas_call(functools.partial(expert_kernel, S, T), out_shape=outs, in...  89.2 us
    pallas_call x1, Pallas kernels, body(): pl.pallas_call(functools.partial(finish_kernel, 8), out_shape=tuple((jax....  3.71 us

profile of v2, /device:TPU:0, one launch (start us, length us, event | category | flops | bytes accessed | tf_op | source)
XLA Modules:
  0.0 93.5 jit_solution(946961859053565480)
XLA Ops:
  0.6 89.2 %experts.1 = (bf16[192,512]{1,0:T(8,128)(2,1)S(1)}, f32[256,128]{1,0:T(8,128)S(1)}, bf16[192,128]{1,0:T(8,128)(2,1)S(1)}, bf16[192,128]{1,0:T(8,128)(2,1)S(1)}, ...) custom-call(s32[2,192]{1,0:T(2,128)} %bitcast.5, ...), custom_call_target="tpu_custom_call" | custom-call | tf_op jit(solution)/shard_map/experts/pallas_call | solution.py:727
  89.8 3.7 %finish.1 = (bf16[192,512]{1,0:T(8,128)(2,1)}, f32[256,128]{1,0:T(8,128)}, bf16[192,128]{1,0:T(8,128)(2,1)}, bf16[192,128]{1,0:T(8,128)(2,1)}, bf16[192,128]{1,0...) custom-call(bf16[192,512]{1,0:T(8,128)(2,1)S(1)} %get-tuple-element.24.refs_0_, ...), custom_call_target="tpu_custom_call" | custom-call | tf_op jit(solution)/shard_map/finish/pallas_call | solution.py:804

commit v3 on v2

--- a/solution.py
+++ b/solution.py
@@ -259,10 +259,21 @@
                 value = value + landed[r - 1, j].astype(F32)
             out[row] = value.astype(BF16)
 
-    lag = 2
+    lag, behind = 3, 7
 
     def block(r):
         return lax.rem(r + 2, S)
+
+    def gathered(r):
+        j = block(r)
+        at = dest(j)
+
+        @pl.when(j != 0)
+        def _():
+            zback(j, True).wait_recv()
+
+        chosen = (slots == code_ref[pl.ds(at, 1), :]).astype(F32).astype(BF16)
+        total_ref[...] += contract_first(chosen, back[at])
 
     def service(t):
         if relay:
@@ -271,13 +282,17 @@
             def _():
                 combine(block(t))
 
-        @pl.when(jnp.logical_and(jnp.logical_and(t >= lag, t < S + lag), t - lag != S - 2))
-        def _():
-            total(block(t - lag), summed, block(t - lag))
-
-        @pl.when(t - lag == S - 2)
-        def _():
-            total(0, back, s)
+        @pl.when(jnp.logical_and(t >= lag, t < S + lag))
+        def _():
+            j = block(t - lag)
+
+            @pl.when(j != 0)
+            def _():
+                total(j, summed, j)
+
+            @pl.when(j == 0)
+            def _():
+                total(j, back, s)
 
         if relay:
 
@@ -286,9 +301,21 @@
                 for h in range(2):
                     bcopy(block(t), h).start()
 
-        @pl.when(jnp.logical_and(t >= lag + 1, t - lag - 1 != S - 2))
-        def _():
-            zback(block(t - lag - 1)).start()
+        @pl.when(jnp.logical_and(t + 2 >= S - 2, t + 2 < S))
+        def _():
+            give(block(t + 2))
+
+        @pl.when(jnp.logical_and(t > lag, t <= S + lag))
+        def _():
+            j = block(t - lag - 1)
+
+            @pl.when(j != 0)
+            def _():
+                zback(j).start()
+
+        @pl.when(jnp.logical_and(t >= behind, t < S + behind))
+        def _():
+            gathered(t - behind)
 
     def give_chunk(q):
         give(2 * q)
@@ -299,6 +326,7 @@
     xg[1, s, :, cols(p)] = zs[1, s]
     pick(1)
     xc[...] = jnp.zeros_like(xc)
+    total_ref[...] = gin_ref[...].astype(F32)
     wait_entry()
     for i in range(2):
         spread(i, 0)
@@ -356,23 +384,87 @@
     def chunk(q):
         return pl.ds(pl.multiple_of(q * 2 * capp, 2 * capp), 2 * capp)
 
+    early = 3
+
+    def message(m):
+        return lax.rem(m // 2, 2), 2 * (m // 4) + lax.rem(m, 2)
+
+    def exchange(q, k):
+        m = 4 * q + k
+
+        @pl.when(m < 4 * n if k % 2 else jnp.logical_and(m > 3, m < 4 * n))
+        def _():
+            forward(*message(m))
+
+        @pl.when(jnp.logical_and(m >= early, m < 4 * n + early))
+        def _():
+            pass_on(*message(m - early))
+
     def step(q):
-        live, later, last = q < n, q > 0, q == n
-
-        @pl.when(jnp.logical_and(live, later))
-        def _():
-            forward(0, 2 * q)
-
-        @pl.when(later)
-        def _():
-            pass_on(1, 2 * q - 1)
+        deep, last, over = q > 1, q == n, q == n + 1
+
+        exchange(q, 0)
+
+        @pl.when(deep)
+        def _():
+            upre[...] = contract_last(xc[0, chunk(q - 2), :], up_w[...])
+
+        @pl.when(over)
+        def _():
+            service(1)
+
+        exchange(q, 1)
+
+        @pl.when(deep)
+        def _():
+            ready(1, q - 2)
+            grad_hidden = contract_last(xc[1, chunk(q - 2), :], down_w[...])
+            gate_pre, up_pre = pre[...], upre[...]
+            sigma = jax.nn.sigmoid(gate_pre)
+            gate_act = gate_pre * sigma
+            hid[chunk(q - 2), :] = (gate_act * up_pre).astype(BF16)
+            gback[chunk(q - 2), :] = (
+                grad_hidden * up_pre * sigma * (1.0 + gate_pre * (1.0 - sigma))
+            ).astype(BF16)
+            uback[chunk(q - 2), :] = (grad_hidden * gate_act).astype(BF16)
+
+        @pl.when(over)
+        def _():
+            service(2)
+
+        exchange(q, 2)
+
+        @pl.when(deep)
+        def _():
+            def piece(f):
+                value = jnp.dot(
+                    gback[chunk(q - 2), :], gate_w[:, cols(f)], preferred_element_type=F32
+                ) + jnp.dot(
+                    uback[chunk(q - 2), :], up_w[:, cols(f)], preferred_element_type=F32
+                )
+                for b in range(2):
+                    part[2 * (q - 2) + b, :, cols(f)] = value[
+                        b * capp : b * capp + cap
+                    ].astype(BF16)
+
+            loop(T, piece)
 
         @pl.when(last)
         def _():
             give_chunk(n - 2)
-            service(0)
-
-        @pl.when(later)
+
+        @pl.when(over)
+        def _():
+            give_chunk(n - 1)
+            service(3)
+
+        exchange(q, 3)
+
+        @pl.when(q == n - 1)
+        def _():
+            loop(n - 3, lambda k: give_chunk(k + 1))
+
+        @pl.when(jnp.logical_and(q > 0, q <= n))
         def _():
             ready(0, q - 1)
 
@@ -383,79 +475,12 @@
 
             pre[...] = contract_last(xc[0, chunk(q - 1), :], gate_w[...])
 
-        @pl.when(live)
-        def _():
-            forward(0, 2 * q + 1)
-            pass_on(0, 2 * q)
-
         @pl.when(last)
         def _():
-            service(1)
-
-        @pl.when(later)
-        def _():
-            upre[...] = contract_last(xc[0, chunk(q - 1), :], up_w[...])
-
-        @pl.when(jnp.logical_and(live, later))
-        def _():
-            forward(1, 2 * q)
-
-        @pl.when(live)
-        def _():
-            pass_on(0, 2 * q + 1)
-
-        @pl.when(last)
-        def _():
-            service(2)
-
-        @pl.when(later)
-        def _():
-            ready(1, q - 1)
-            grad_hidden = contract_last(xc[1, chunk(q - 1), :], down_w[...])
-            gate_pre, up_pre = pre[...], upre[...]
-            sigma = jax.nn.sigmoid(gate_pre)
-            gate_act = gate_pre * sigma
-            hid[chunk(q - 1), :] = (gate_act * up_pre).astype(BF16)
-            gback[chunk(q - 1), :] = (
-                grad_hidden * up_pre * sigma * (1.0 + gate_pre * (1.0 - sigma))
-            ).astype(BF16)
-            uback[chunk(q - 1), :] = (grad_hidden * gate_act).astype(BF16)
-
-        @pl.when(live)
-        def _():
-            forward(1, 2 * q + 1)
-            pass_on(1, 2 * q)
-
-        @pl.when(last)
-        def _():
-            service(3)
-
-        @pl.when(later)
-        def _():
-            def piece(f):
-                value = jnp.dot(
-                    gback[chunk(q - 1), :], gate_w[:, cols(f)], preferred_element_type=F32
-                ) + jnp.dot(
-                    uback[chunk(q - 1), :], up_w[:, cols(f)], preferred_element_type=F32
-                )
-                for b in range(2):
-                    part[2 * (q - 1) + b, :, cols(f)] = value[
-                        b * capp : b * capp + cap
-                    ].astype(BF16)
-
-            loop(T, piece)
-
-        @pl.when(q == n - 1)
-        def _():
-            loop(n - 3, lambda k: give_chunk(k + 1))
-
-        @pl.when(last)
-        def _():
-            give_chunk(n - 1)
-            give_chunk(0)
+            service(0)
 
     send_edges(0)
-    loop(n + 1, step)
+    loop(n + 2, step)
 
     for load in loads[9:]:
         load.wait()
@@ -486,8 +511,8 @@
                     left[...], xc[i, :, at], preferred_element_type=F32
                 ).astype(BF16)
 
-    steps = S + lag + 1 - 4
-    each = -(-3 * tiles // (steps - 1))
+    steps = S + behind - 4
+    each = 2 if relay else -(-3 * tiles // steps)
 
     def finish_step(t):
         for k in range(each):
@@ -500,20 +525,6 @@
 
     loop(steps, finish_step)
 
-    total_ref[...] = gin_ref[...].astype(F32)
-
-    def gathered(r):
-        j = block(r)
-        at = dest(j)
-
-        @pl.when(j != 0)
-        def _():
-            zback(j, True).wait_recv()
-
-        chosen = (slots == code_ref[pl.ds(at, 1), :]).astype(F32).astype(BF16)
-        total_ref[...] += contract_first(chosen, back[at])
-
-    loop(S, gathered)
     value = total_ref[...].astype(BF16)
     own_ref[...] = value
     full_ref[:, cols(p)] = value

time: 95.4 us -> 94.1 us (0.986); the launches traced: 93.5 us -> 93.9 us
  no operation moved by 1% of the time
where the time goes in v3:
time: 94.1 us; the launch traced here: 93.9 us
  Pallas kernels  93.3 us (99%)
    pallas_call x1, Pallas kernels, body(): pl.pallas_call(functools.partial(expert_kernel, S, T), out_shape=outs, in...  89.6 us
    pallas_call x1, Pallas kernels, body(): pl.pallas_call(functools.partial(finish_kernel, 8), out_shape=tuple((jax....  3.71 us

profile of v3, /device:TPU:0, one launch (start us, length us, event | category | flops | bytes accessed | tf_op | source)
XLA Modules:
  0.0 93.9 jit_solution(14411037667816878430)
XLA Ops:
  0.6 89.6 %experts.1 = (bf16[192,512]{1,0:T(8,128)(2,1)S(1)}, f32[256,128]{1,0:T(8,128)S(1)}, bf16[192,128]{1,0:T(8,128)(2,1)S(1)}, bf16[192,128]{1,0:T(8,128)(2,1)S(1)}, ...) custom-call(s32[2,192]{1,0:T(2,128)} %bitcast.5, ...), custom_call_target="tpu_custom_call" | custom-call | tf_op jit(solution)/shard_map/experts/pallas_call | solution.py:738
  90.2 3.7 %finish.1 = (bf16[192,512]{1,0:T(8,128)(2,1)}, f32[256,128]{1,0:T(8,128)}, bf16[192,128]{1,0:T(8,128)(2,1)}, bf16[192,128]{1,0:T(8,128)(2,1)}, bf16[192,128]{1,0...) custom-call(bf16[192,512]{1,0:T(8,128)(2,1)S(1)} %get-tuple-element.24.refs_0_, ...), custom_call_target="tpu_custom_call" | custom-call | tf_op jit(solution)/shard_map/finish/pallas_call | solution.py:815

commit v4 on v3

--- a/solution.py
+++ b/solution.py
@@ -259,7 +259,7 @@
                 value = value + landed[r - 1, j].astype(F32)
             out[row] = value.astype(BF16)
 
-    lag, behind = 3, 7
+    lag, behind = 2, 8
 
     def block(r):
         return lax.rem(r + 2, S)
@@ -301,9 +301,9 @@
                 for h in range(2):
                     bcopy(block(t), h).start()
 
-        @pl.when(jnp.logical_and(t + 2 >= S - 2, t + 2 < S))
-        def _():
-            give(block(t + 2))
+        @pl.when(t == S - 4)
+        def _():
+            give_chunk(0)
 
         @pl.when(jnp.logical_and(t > lag, t <= S + lag))
         def _():
@@ -318,8 +318,14 @@
             gathered(t - behind)
 
     def give_chunk(q):
-        give(2 * q)
-        give(2 * q + 1)
+        if relay:
+            for k in (1, 0):
+                for b in range(2):
+                    for h in range(2):
+                        tcopy(2 * q + b, h, k).start()
+        else:
+            give(2 * q)
+            give(2 * q + 1)
 
     pick(0)
     xg[0, s, :, cols(p)] = zs[0, s]

time: 94.1 us -> 93 us (0.988)
  Pallas kernels: 93.3 us -> 91.9 us
    pallas_call x1, Pallas kernels: 89.6 us -> 88.2 us  [body(): pl.pallas_call(functools.partial(expert_kernel, S, T), out_shape=outs, in...]
where the time goes in v4:
time: 93 us; the launch traced here: 92.6 us
  Pallas kernels  91.9 us (99%)
    pallas_call x1, Pallas kernels, body(): pl.pallas_call(functools.partial(expert_kernel, S, T), out_shape=outs, in...  88.2 us
    pallas_call x1, Pallas kernels, body(): pl.pallas_call(functools.partial(finish_kernel, 8), out_shape=tuple((jax....  3.71 us

profile of v4, /device:TPU:0, one launch (start us, length us, event | category | flops | bytes accessed | tf_op | source)
XLA Modules:
  0.0 92.6 jit_solution(7453456565131594778)
XLA Ops:
  0.6 88.2 %experts.1 = (bf16[192,512]{1,0:T(8,128)(2,1)S(1)}, f32[256,128]{1,0:T(8,128)S(1)}, bf16[192,128]{1,0:T(8,128)(2,1)S(1)}, bf16[192,128]{1,0:T(8,128)(2,1)S(1)}, ...) custom-call(s32[2,192]{1,0:T(2,128)} %bitcast.5, ...), custom_call_target="tpu_custom_call" | custom-call | tf_op jit(solution)/shard_map/experts/pallas_call | solution.py:744
  88.9 3.7 %finish.1 = (bf16[192,512]{1,0:T(8,128)(2,1)}, f32[256,128]{1,0:T(8,128)}, bf16[192,128]{1,0:T(8,128)(2,1)}, bf16[192,128]{1,0:T(8,128)(2,1)}, bf16[192,128]{1,0...) custom-call(bf16[192,512]{1,0:T(8,128)(2,1)S(1)} %get-tuple-element.24.refs_0_, ...), custom_call_target="tpu_custom_call" | custom-call | tf_op jit(solution)/shard_map/finish/pallas_call | solution.py:821
